TPU v7x, 32 devices: a whole 2x2x4 slice. The times are simulated.
32 devices in a mesh: fs: 8 (over z, y), tp: 4 (over x, core).
Axes of the slice: x: 2, y: 2, z: 4, core: 2. Of those that a mesh axis runs over, the one named last changes fastest.
Arguments:
- tokens: bfloat16 [8192, 2048], P('fs', 'tp'), may hold values from -6 to 6
- norm_gain: float32 [2048], P('fs'), may hold values from 0.1 to 1.9
- up_master: float32 [2048, 4096], P('fs', 'tp'), may hold values from -0.125 to 0.125
- down_master: float32 [4096, 2048], P('fs', 'tp'), may hold values from -0.09375 to 0.09375
Outputs:
- mixed: bfloat16 [8192, 2048], P('fs', 'tp')
- up_ready: bfloat16 [2048, 4096], P(None, 'tp')
- down_ready: bfloat16 [4096, 2048], P('tp')
All inputs are finite; a program needn't handle non-finite values.
Results may differ from a plain program's by a relative error of at most 0.0095.
Values may be sent and summed in bfloat16 or wider, within the bound.
A program may use at most 128 MiB of HBM per device.

v0:
```python
import functools

import jax
import jax.numpy as jnp
from jax import lax
from jax.experimental import pallas as pl
from jax.experimental.pallas import tpu as pltpu
from jax.sharding import PartitionSpec as P

UP_CUTS = 2
DOWN_CUTS = 2
COLUMNS = 256
LANES = 128
VMEM_LIMIT = 40
MIB = 1024 * 1024


def kernel(
    n, n_tp,
    tokens_hbm, gain_hbm, upm_hbm, downm_hbm,
    up, down, own, take, crossed,
    gain_in, upm_in, downm_in, tok, shard, scale, hidden, kept, give, cross,
    tok_send, tok_recv, gather_send, gather_recv,
    up_send, upz_recv, upy_recv, both_send, both_recv,
    down_send, downz_recv, downy_recv,
    pair_send, pair_recv, cross_send, cross_recv, local_sem,
):
    f32, bf16 = jnp.float32, jnp.bfloat16
    f, t = lax.axis_index("fs"), lax.axis_index("tp")
    lines = n // 2
    z, y = f // 2, f % 2
    t1 = t + 1 - 2 * (t % 2)
    t2 = (t + 2) % 4
    t3 = (t1 + 2) % 4
    members = n // n_tp
    starts = members // 2
    owner = f // members
    above, below = (f + 2) % n, (f + n - 2) % n
    across = f + 1 - 2 * y
    has_above, has_below = z < lines - 1, z > 0

    up_rows = upm_in.shape[0]
    down_rows = downm_in.shape[0]
    feats = tokens_hbm.shape[1]
    dcut = down_rows // DOWN_CUTS
    first_cut = max(8, up_rows // 8)
    ucuts = (first_cut, first_cut + (up_rows - first_cut) // 16 * 8, up_rows)

    def remote(src, dst, send, recv, **to):
        return pltpu.make_async_remote_copy(
            src_ref=src, dst_ref=dst, send_sem=send, recv_sem=recv,
            device_id=to, device_id_type=pl.DeviceIdType.MESH,
        )

    def down_block(source, column):
        rows = pl.ds(pl.multiple_of(source % members * down_rows, down_rows), down_rows)
        return down.at[rows, pl.ds(pl.multiple_of(column * feats, feats), feats)]

    loads = [
        pltpu.make_async_copy(upm_hbm, upm_in, local_sem.at[0]),
        pltpu.make_async_copy(gain_hbm, gain_in, local_sem.at[1]),
        pltpu.make_async_copy(downm_hbm, downm_in, local_sem.at[2]),
        pltpu.make_async_copy(
            tokens_hbm, tok.at[:, pl.ds(pl.multiple_of(t * feats, feats), feats)],
            local_sem.at[3],
        ),
    ]
    for load in loads:
        load.start()

    barrier = pltpu.get_barrier_semaphore()
    for other in (t1, t2, t3):
        pl.semaphore_signal(
            barrier, inc=1, device_id={"tp": other}, device_id_type=pl.DeviceIdType.MESH
        )
    pl.semaphore_signal(
        barrier, inc=1, device_id={"fs": across}, device_id_type=pl.DeviceIdType.MESH
    )

    @pl.when(has_above)
    def _():
        pl.semaphore_signal(
            barrier, inc=1, device_id={"fs": above}, device_id_type=pl.DeviceIdType.MESH
        )

    @pl.when(has_below)
    def _():
        pl.semaphore_signal(
            barrier, inc=1, device_id={"fs": below}, device_id_type=pl.DeviceIdType.MESH
        )

    loads[0].wait()
    loads[1].wait()
    gain = jnp.transpose(jnp.broadcast_to(gain_in[...], (LANES, up_rows)))
    for first in range(0, up.shape[1], LANES):
        up[pl.ds(pl.multiple_of(f * up_rows, up_rows), up_rows), pl.ds(first, LANES)] = (
            gain * upm_in[:, pl.ds(first, LANES)]
        ).astype(bf16)

    loads[2].wait()
    shard[...] = downm_in[...].astype(bf16)

    @pl.when(owner == t)
    def _():
        down_block(f, t)[...] = downm_in[...].astype(bf16)

    pl.semaphore_wait(
        barrier, 4 + has_above.astype(jnp.int32) + has_below.astype(jnp.int32)
    )

    def up_piece(line, column, u):
        first, last = (ucuts[u], ucuts[u + 1]) if u >= 0 else (0, ucuts[0])
        row = (line * 2 + column) * up_rows + first
        return up.at[pl.ds(pl.multiple_of(row, 8), last - first), :]

    def both_copy(way, line, column, to):
        piece = up_piece(line, column, -1)
        return remote(
            piece, piece, both_send.at[way, line, column], both_recv.at[line, column], fs=to
        )

    def both_onward(line, column, start):
        def go(copy):
            copy.start() if start else copy.wait_send()

        @pl.when(has_above & (line <= z))
        def _():
            go(both_copy(0, line, column, above))

        @pl.when(has_below & (line >= z))
        def _():
            go(both_copy(1, line, column, below))

    def up_copy(way, line, u, to):
        piece = up_piece(line, y, u)
        recv = upy_recv if way == 2 else upz_recv
        return remote(piece, piece, up_send.at[way, line, u], recv.at[line, u], fs=to)

    def up_onward(line, u, start):
        def go(copy):
            copy.start() if start else copy.wait_send()

        @pl.when(has_above & (line <= z))
        def _():
            go(up_copy(0, line, u, above))

        @pl.when(has_below & (line >= z))
        def _():
            go(up_copy(1, line, u, below))

        go(up_copy(2, line, u, across))

    both_copy(2, z, y, across).start()
    both_onward(z, y, True)
    for u in range(UP_CUTS):
        up_onward(z, u, True)

    def gather_copy(column, to):
        return remote(
            shard, down_block(f, column), gather_send.at[0], gather_recv.at[column], tp=to
        )

    @pl.when(owner != t)
    def _():
        gather_copy(t, owner).start()

    loads[3].wait()

    def tok_copy(way, column, to):
        piece = tok.at[:, pl.ds(pl.multiple_of(column * feats, feats), feats)]
        return remote(piece, piece, tok_send.at[way], tok_recv.at[way], tp=to)

    tok_copy(1, t, t2).start()
    tok_copy(0, t, t1).start()

    both_copy(2, z, 1 - y, across).wait_recv()
    both_onward(z, 1 - y, True)

    def both_relay(line, column):
        @pl.when((line >= 0) & (line < lines))
        def _():
            both_copy(0, line, column, above).wait_recv()
            both_onward(line, column, True)

    @pl.loop(1, lines)
    def _(d):
        both_relay(z - d, y)
        both_relay(z + d, y)
        for u in range(UP_CUTS):
            @pl.when(z - d >= 0)
            def _():
                up_copy(0, z - d, u, above).wait_recv()
                up_onward(z - d, u, True)

            @pl.when(z + d < lines)
            def _():
                up_copy(1, z + d, u, below).wait_recv()
                up_onward(z + d, u, True)

        both_relay(z - d, 1 - y)
        both_relay(z + d, 1 - y)

    tok_copy(1, t2, t2).wait_recv()
    tok_copy(2, t2, t1).start()

    half = feats // 2
    order = ((t2, 0), (t3, 0), (t2, 1), (t3, 1), (t1, 0), (t1, 1), (t, 0), (t, 1))

    def down_piece(ci, js, side, q):
        column, part = order[ci]
        line = t * starts + js
        row = ((line * 2 + side) % members) * down_rows + q * dcut
        return down.at[
            pl.ds(pl.multiple_of(row, dcut), dcut),
            pl.ds(pl.multiple_of(column * feats + part * half, half), half),
        ]

    def down_copy(way, ci, js, q, to):
        piece = down_piece(ci, js, y, q)
        recv = downy_recv if way == 2 else downz_recv
        return remote(
            piece, piece, down_send.at[way, ci, js, q], recv.at[ci, js, q], fs=to
        )

    def down_onward(ci, js, q, start):
        line = t * starts + js

        def go(copy):
            copy.start() if start else copy.wait_send()

        @pl.when(has_above & (line <= z))
        def _():
            go(down_copy(0, ci, js, q, above))

        @pl.when(has_below & (line >= z))
        def _():
            go(down_copy(1, ci, js, q, below))

        go(down_copy(2, ci, js, q, across))

    def relay(ci, q):
        @pl.loop(0, starts)
        def _(js):
            line = t * starts + js

            if q == 0 and ci in (0, 1, 4):
                @pl.when(line == z)
                def _():
                    gather_copy(order[ci][0], t).wait_recv()

            @pl.when(line != z)
            def _():
                down_copy(0, ci, js, q, above).wait_recv()

            down_onward(ci, js, q, True)

    def relayed(ci):
        @pl.loop(0, starts)
        def _(js):
            for q in range(DOWN_CUTS):
                piece = down_piece(ci, js, 1 - y, q)
                remote(
                    piece, piece, down_send.at[2, ci, js, q], downy_recv.at[ci, js, q],
                    fs=across,
                ).wait_recv()

    for ci in (0, 1):
        for q in range(DOWN_CUTS):
            relay(ci, q)

    tok_copy(0, t1, t1).wait_recv()
    tok_copy(2, t3, t1).wait_recv()

    rows_all = tok.shape[0]
    step = min(rows_all, 128)

    @pl.loop(0, rows_all // step)
    def _(i):
        rows = pl.ds(pl.multiple_of(i * step, step), step)
        values = tok[rows, :].astype(f32)
        mean_square = jnp.mean(values * values, axis=-1, keepdims=True)
        scale[rows, :] = lax.rsqrt(mean_square + 1e-06)

    @pl.loop(0, lines)
    def _(line):
        for u in range(UP_CUTS):
            piece = up_piece(line, 1 - y, u)
            remote(
                piece, piece, up_send.at[2, line, u], upy_recv.at[line, u], fs=across
            ).wait_recv()

    width = up.shape[1]
    tiles = width // COLUMNS
    for q in range(DOWN_CUTS):
        relay(2, q)

        @pl.loop(q * tiles // DOWN_CUTS, (q + 1) * tiles // DOWN_CUTS)
        def _(i):
            columns = pl.ds(pl.multiple_of(i * COLUMNS, COLUMNS), COLUMNS)
            before = jnp.dot(tok[...], up[:, columns], preferred_element_type=f32)
            value = jnp.maximum(before * scale[...], 0.0)
            hidden[:, columns] = (value * value).astype(bf16)

    def product(ci):
        column, part = order[ci]
        first = pl.multiple_of(column * feats + part * half, half)
        return jnp.dot(hidden[...], down[:, pl.ds(first, half)], preferred_element_type=f32)

    def pair_copy(i):
        return remote(give.at[i], take.at[i], pair_send.at[i], pair_recv.at[i], tp=t1)

    def cross_copy(i):
        return remote(
            cross.at[i], crossed.at[i], cross_send.at[i], cross_recv.at[i], tp=t2
        )

    def cross_over(i):
        pair_copy(i).wait_recv()

        @pl.loop(0, rows_all // step)
        def _(j):
            rows = pl.ds(pl.multiple_of(j * step, step), step)
            cross[i, rows, :] = (kept[rows, :] + take[i, rows, :].astype(f32)).astype(bf16)

        cross_copy(i).start()

    relay(3, 0)
    relayed(0)
    kept[...] = product(0)
    for q in range(1, DOWN_CUTS):
        relay(3, q)
    relayed(1)
    give[0] = product(1).astype(bf16)
    pair_copy(0).start()
    relay(4, 0)
    cross_over(0)
    for q in range(1, DOWN_CUTS):
        relay(4, q)
    relayed(2)
    kept[...] = product(2)
    for q in range(DOWN_CUTS):
        relay(5, q)
    relayed(3)
    give[1] = product(3).astype(bf16)
    pair_copy(1).start()
    relay(6, 0)
    cross_over(1)
    for q in range(1, DOWN_CUTS):
        relay(6, q)
    for q in range(DOWN_CUTS):
        relay(7, q)
    for ci, i in ((4, 2), (5, 3)):
        relayed(ci)
        give[i] = product(ci).astype(bf16)
        pair_copy(i).start()
    for i in range(2):
        relayed(6 + i)
        own[i] = product(6 + i)
        pair_copy(2 + i).wait_recv()
        cross_copy(i).wait_recv()

    @pl.loop(0, lines)
    def _(line):
        for u in range(UP_CUTS):
            up_onward(line, u, False)
        for column in range(2):
            both_onward(line, column, False)

    both_copy(2, z, y, across).wait_send()

    @pl.loop(0, starts)
    def _(js):
        for ci in range(len(order)):
            for q in range(DOWN_CUTS):
                down_onward(ci, js, q, False)

    @pl.when(owner != t)
    def _():
        gather_copy(t, owner).wait_send()

    tok_copy(0, t, t1).wait_send()
    tok_copy(1, t, t2).wait_send()
    tok_copy(2, t2, t1).wait_send()
    for i in range(4):
        pair_copy(i).wait_send()
    for i in range(2):
        cross_copy(i).wait_send()


def finish(up, down, own, take, crossed, mixed_hbm, up_hbm, down_hbm, mixed, sems):
    copies = [
        pltpu.make_async_copy(up, up_hbm, sems.at[0]),
        pltpu.make_async_copy(down, down_hbm, sems.at[1]),
    ]
    for copy in copies:
        copy.start()
    rows_all, half = own.shape[1:]
    step = min(rows_all, 128)
    for i in range(2):
        @pl.loop(0, rows_all // step)
        def _(j):
            rows = pl.ds(pl.multiple_of(j * step, step), step)
            mixed[rows, pl.ds(i * half, half)] = (
                own[i, rows, :] + take[2 + i, rows, :].astype(jnp.float32)
                + crossed[i, rows, :].astype(jnp.float32)
            ).astype(mixed.dtype)

    copies.append(pltpu.make_async_copy(mixed, mixed_hbm, sems.at[2]))
    copies[2].start()
    for copy in copies:
        copy.wait()


def fused(n, n_tp, tokens, norm_gain, up_master, down_master):
    rows, feats = tokens.shape
    up_rows, width = up_master.shape
    down_rows = down_master.shape[0]
    depth = up_rows * n
    model = feats * n_tp
    half = feats // 2
    lines, starts = n // 2, n // n_tp // 2
    bf16, f32 = jnp.bfloat16, jnp.float32
    dma = pltpu.SemaphoreType.DMA
    vmem = pl.BlockSpec(memory_space=pltpu.VMEM)
    hbm = pl.BlockSpec(memory_space=pltpu.HBM)
    flops = 4 * rows * depth * width
    kept = pl.pallas_call(
        functools.partial(kernel, n, n_tp),
        out_shape=(
            pltpu.VMEM((depth, width), bf16),
            pltpu.VMEM((width, model), bf16),
            pltpu.VMEM((2, rows, half), f32),
            pltpu.VMEM((4, rows, half), bf16),
            pltpu.VMEM((2, rows, half), bf16),
        ),
        in_specs=[hbm] * 4,
        out_specs=(vmem,) * 5,
        scratch_shapes=[
            pltpu.VMEM((1, up_rows), f32),
            pltpu.VMEM(up_master.shape, f32),
            pltpu.VMEM(down_master.shape, f32),
            pltpu.VMEM((rows, model), bf16),
            pltpu.VMEM((down_rows, feats), bf16),
            pltpu.VMEM((rows, 1), f32),
            pltpu.VMEM((rows, width), bf16),
            pltpu.VMEM((rows, half), f32),
            pltpu.VMEM((4, rows, half), bf16),
            pltpu.VMEM((2, rows, half), bf16),
            dma((3,)), dma((3,)), dma((1,)), dma((n_tp,)),
            dma((3, lines, UP_CUTS)), dma((lines, UP_CUTS)), dma((lines, UP_CUTS)),
            dma((3, lines, 2)), dma((lines, 2)),
            dma((3, 8, starts, DOWN_CUTS)),
            dma((8, starts, DOWN_CUTS)), dma((8, starts, DOWN_CUTS)),
            dma((4,)), dma((4,)), dma((2,)), dma((2,)), dma((4,)),
        ],
        compiler_params=pltpu.CompilerParams(
            collective_id=0, has_side_effects=True, vmem_limit_bytes=VMEM_LIMIT * MIB
        ),
        cost_estimate=pl.CostEstimate(flops=flops, bytes_accessed=16 * MIB, transcendentals=0),
        name="layer",
    )(tokens, norm_gain[None, :], up_master, down_master)
    return pl.pallas_call(
        finish,
        out_shape=(
            jax.ShapeDtypeStruct((rows, feats), bf16),
            jax.ShapeDtypeStruct((depth, width), bf16),
            jax.ShapeDtypeStruct((width, model), bf16),
        ),
        in_specs=[vmem] * 5,
        out_specs=(hbm,) * 3,
        scratch_shapes=[pltpu.VMEM((rows, feats), bf16), dma((3,))],
        compiler_params=pltpu.CompilerParams(vmem_limit_bytes=8 * MIB),
        name="finish",
    )(*kept)


def solution(mesh):
    n, n_tp = mesh.shape["fs"], mesh.shape["tp"]
    return jax.shard_map(
        functools.partial(fused, n, n_tp),
        mesh=mesh,
        in_specs=(P("fs", "tp"), P("fs"), P("fs", "tp"), P("fs", "tp")),
        out_specs=(P("fs", "tp"), P(None, "tp"), P("tp", None)),
        check_vma=False,
    )
```

profile of v0, /device:TPU:0, one launch (start us, length us, event | category | flops | bytes accessed | tf_op | source)
XLA Modules:
  0.0 106.7 jit_solution(13063210466923664655)
XLA Ops:
  0.6 0.0 copy-start
  0.6 0.7 copy-done
  1.3 101.7 %layer.1 = (bf16[2048,1024]{1,0:T(8,128)(2,1)S(1)}, bf16[1024,2048]{1,0:T(8,128)(2,1)S(1)}, f32[2,1024,256]{2,1,0:T(8,128)S(1)}, bf16[4,1024,256]{2,1,0:T(8,128)(2,1)S(1)}, bf16[2,1024,256]{2,1,0:T(8,128)(2,1)S(1)}) custom-call(bf16[1024,512]{1,0:T(8,128)(2,1)} %tokens_hbm.1, f32[1,256]{1,0:T(1,128)S(1)} %bitcast.1, f32[256,1024]{1,0:T(8,128)} %upm_hbm.1, ...), custom_call_target="tpu_custom_call" | custom-call | flops 8589934592 | bytes 16777216 | tf_op jit(solution)/shard_map/layer/pallas_call | solution.py:427
  103.1 3.6 %finish.1 = (bf16[1024,512]{1,0:T(8,128)(2,1)}, bf16[2048,1024]{1,0:T(8,128)(2,1)}, bf16[1024,2048]{1,0:T(8,128)(2,1)}) custom-call(bf16[2048,1024]{1,0:T(8,128)(2,1)S(1)} %get-tuple-element.8.up, bf16[1024,2048]{1,0:T(8,128)(2,1)S(1)} %get-tuple-element.9.down, f32[2,1024,256]{2,1,0:T(8,128)S(1)} %get-tuple-element.10.own, ...), custom_call_target="tpu_custom_call" | custom-call | tf_op jit(solution)/shard_map/finish/pallas_call | solution.py:462
Async XLA Ops:
  0.6 0.7 copy-start
where the time goes:
time: 107 us
  Pallas kernels  105 us (98%)
    pallas_call x1, Pallas kernels, fused(): pl.pallas_call(functools.partial(kernel, n, n_tp), out_shape=(pltpu.VMEM(...  102 us
    pallas_call x1, Pallas kernels, fused(): pl.pallas_call(finish, out_shape=(jax.ShapeDtypeStruct((rows, feats), bf1...  3.64 us

commit v1 on v0

--- a/solution.py
+++ b/solution.py
@@ -10,6 +10,7 @@
 UP_CUTS = 2
 DOWN_CUTS = 2
 COLUMNS = 256
+BOTH = 3
 LANES = 128
 VMEM_LIMIT = 40
 MIB = 1024 * 1024
@@ -19,10 +20,10 @@
     n, n_tp,
     tokens_hbm, gain_hbm, upm_hbm, downm_hbm,
     up, down, own, take, crossed,
-    gain_in, upm_in, downm_in, tok, shard, scale, hidden, kept, give, cross,
+    gain_in, upm_in, downm_in, tok, shard, passing, scale, hidden, kept, give, cross,
     tok_send, tok_recv, gather_send, gather_recv,
     up_send, upz_recv, upy_recv, both_send, both_recv,
-    down_send, downz_recv, downy_recv,
+    down_send, downz_recv, downy_recv, pass_send, pass_recv, last_send, last_recv,
     pair_send, pair_recv, cross_send, cross_recv, local_sem,
 ):
     f32, bf16 = jnp.float32, jnp.bfloat16
@@ -38,12 +39,15 @@
     above, below = (f + 2) % n, (f + n - 2) % n
     across = f + 1 - 2 * y
     has_above, has_below = z < lines - 1, z > 0
+    upper, lower = t >= n_tp // 2, t < n_tp // 2
+    at_end = jnp.logical_not(has_above & has_below)
 
     up_rows = upm_in.shape[0]
     down_rows = downm_in.shape[0]
     feats = tokens_hbm.shape[1]
+    half = feats // 2
     dcut = down_rows // DOWN_CUTS
-    first_cut = max(8, up_rows // 8)
+    first_cut = max(8, up_rows * BOTH // 128 * 8)
     ucuts = (first_cut, first_cut + (up_rows - first_cut) // 16 * 8, up_rows)
 
     def remote(src, dst, send, recv, **to):
@@ -98,11 +102,18 @@
         ).astype(bf16)
 
     loads[2].wait()
-    shard[...] = downm_in[...].astype(bf16)
 
     @pl.when(owner == t)
     def _():
         down_block(f, t)[...] = downm_in[...].astype(bf16)
+
+    @pl.when(owner == t2)
+    def _():
+        passing[z % starts] = downm_in[...].astype(bf16)
+
+    @pl.when((owner == t1) | (owner == t3))
+    def _():
+        shard[...] = downm_in[...].astype(bf16)
 
     pl.semaphore_wait(
         barrier, 4 + has_above.astype(jnp.int32) + has_below.astype(jnp.int32)
@@ -119,17 +130,17 @@
             piece, piece, both_send.at[way, line, column], both_recv.at[line, column], fs=to
         )
 
+    def run(copy, start):
+        copy.start() if start else copy.wait_send()
+
     def both_onward(line, column, start):
-        def go(copy):
-            copy.start() if start else copy.wait_send()
-
         @pl.when(has_above & (line <= z))
         def _():
-            go(both_copy(0, line, column, above))
+            run(both_copy(0, line, column, above), start)
 
         @pl.when(has_below & (line >= z))
         def _():
-            go(both_copy(1, line, column, below))
+            run(both_copy(1, line, column, below), start)
 
     def up_copy(way, line, u, to):
         piece = up_piece(line, y, u)
@@ -137,18 +148,15 @@
         return remote(piece, piece, up_send.at[way, line, u], recv.at[line, u], fs=to)
 
     def up_onward(line, u, start):
-        def go(copy):
-            copy.start() if start else copy.wait_send()
-
         @pl.when(has_above & (line <= z))
         def _():
-            go(up_copy(0, line, u, above))
+            run(up_copy(0, line, u, above), start)
 
         @pl.when(has_below & (line >= z))
         def _():
-            go(up_copy(1, line, u, below))
-
-        go(up_copy(2, line, u, across))
+            run(up_copy(1, line, u, below), start)
+
+        run(up_copy(2, line, u, across), start)
 
     both_copy(2, z, y, across).start()
     both_onward(z, y, True)
@@ -160,10 +168,70 @@
             shard, down_block(f, column), gather_send.at[0], gather_recv.at[column], tp=to
         )
 
-    @pl.when(owner != t)
+    order = ((t3, 0), (t2, 0), (t3, 1), (t2, 1), (t1, 0), (t1, 1), (t, 0), (t, 1))
+    passed = (1, 3)
+    finals = 7
+    early = (0, 1, 2)
+
+    def pass_copies(part, js, q, start, ways=(0, 1)):
+        line = t2 * starts + js
+        row = ((line * 2 + y) % members) * down_rows + q * dcut
+        ci = passed[part]
+        here = passing.at[js, pl.ds(q * dcut, dcut), pl.ds(part * half, half)]
+        there = down.at[
+            pl.ds(pl.multiple_of(row, dcut), dcut),
+            pl.ds(pl.multiple_of(t * feats + part * half, half), half),
+        ]
+
+        def onward(to):
+            return remote(
+                here, here, pass_send.at[0, part, js, q], pass_recv.at[part, js, q], fs=to
+            )
+
+        if 0 in ways:
+            @pl.when(lower & has_below & (line >= z))
+            def _():
+                run(onward(below), start)
+
+            @pl.when(upper & has_above & (line <= z))
+            def _():
+                run(onward(above), start)
+
+        if 1 in ways:
+            @pl.when((upper & (line <= z)) | (lower & (line >= z)))
+            def _():
+                over = remote(
+                    here, there, pass_send.at[1, part, js, q], downz_recv.at[ci, js, q],
+                    tp=t2,
+                )
+                run(over, start)
+
+    def pass_on(part, q):
+        @pl.loop(0, starts)
+        def _(js):
+            line = t2 * starts + js
+
+            @pl.when((upper & (line < z)) | (lower & (line > z)))
+            def _():
+                here = passing.at[js, pl.ds(q * dcut, dcut), pl.ds(part * half, half)]
+                remote(
+                    here, here, pass_send.at[0, part, js, q], pass_recv.at[part, js, q],
+                    fs=above,
+                ).wait_recv()
+                pass_copies(part, js, q, True)
+
+    def pass_start(way):
+        @pl.when(owner == t2)
+        def _():
+            for part in range(2):
+                for q in range(DOWN_CUTS):
+                    pass_copies(part, z % starts, q, True, (way,))
+
+    @pl.when((owner == t1) | (owner == t3))
     def _():
         gather_copy(t, owner).start()
 
+    pass_start(1)
     loads[3].wait()
 
     def tok_copy(way, column, to):
@@ -181,30 +249,6 @@
         def _():
             both_copy(0, line, column, above).wait_recv()
             both_onward(line, column, True)
-
-    @pl.loop(1, lines)
-    def _(d):
-        both_relay(z - d, y)
-        both_relay(z + d, y)
-        for u in range(UP_CUTS):
-            @pl.when(z - d >= 0)
-            def _():
-                up_copy(0, z - d, u, above).wait_recv()
-                up_onward(z - d, u, True)
-
-            @pl.when(z + d < lines)
-            def _():
-                up_copy(1, z + d, u, below).wait_recv()
-                up_onward(z + d, u, True)
-
-        both_relay(z - d, 1 - y)
-        both_relay(z + d, 1 - y)
-
-    tok_copy(1, t2, t2).wait_recv()
-    tok_copy(2, t2, t1).start()
-
-    half = feats // 2
-    order = ((t2, 0), (t3, 0), (t2, 1), (t3, 1), (t1, 0), (t1, 1), (t, 0), (t, 1))
 
     def down_piece(ci, js, side, q):
         column, part = order[ci]
@@ -222,37 +266,127 @@
             piece, piece, down_send.at[way, ci, js, q], recv.at[ci, js, q], fs=to
         )
 
-    def down_onward(ci, js, q, start):
+    def down_lines(ci, js, q, start):
         line = t * starts + js
-
-        def go(copy):
-            copy.start() if start else copy.wait_send()
-
-        @pl.when(has_above & (line <= z))
-        def _():
-            go(down_copy(0, ci, js, q, above))
-
-        @pl.when(has_below & (line >= z))
-        def _():
-            go(down_copy(1, ci, js, q, below))
-
-        go(down_copy(2, ci, js, q, across))
-
-    def relay(ci, q):
+        rising = has_above & (line <= z)
+        falling = has_below & (line >= z)
+        if ci in passed:
+            rising = rising & upper
+            falling = falling & lower
+        elif start:
+            rising = rising & (upper | (line < z))
+            falling = falling & (lower | (line > z))
+
+        @pl.when(rising)
+        def _():
+            run(down_copy(0, ci, js, q, above), start)
+
+        @pl.when(falling)
+        def _():
+            run(down_copy(1, ci, js, q, below), start)
+
+    def down_over(ci, js, q, start):
+        line = t * starts + js
+        if ci == finals:
+            @pl.when(line == z)
+            def _():
+                run(down_copy(2, ci, js, q, across), start)
+        elif start and ci in early:
+            @pl.when(line != z)
+            def _():
+                down_copy(2, ci, js, q, across).start()
+        else:
+            run(down_copy(2, ci, js, q, across), start)
+
+    def far_start():
+        js = z % starts
+
+        def send(make):
+            @pl.when(lower & has_above)
+            def _():
+                make(0, above).start()
+
+            @pl.when(upper & has_below)
+            def _():
+                make(1, below).start()
+
+        @pl.when(owner == t)
+        def _():
+            for ci in (0, 2, 4, 5, 6):
+                for q in range(DOWN_CUTS):
+                    send(lambda way, to: down_copy(way, ci, js, q, to))
+            for q in range(DOWN_CUTS):
+                send(lambda way, to: last_copy(way, js, y, q, to))
+
+    def last_copy(way, js, side, q, to):
+        piece = down_piece(finals, js, side, q)
+        return remote(
+            piece, piece, last_send.at[way, js, side, q], last_recv.at[js, side, q], fs=to
+        )
+
+    def last_onward(js, side, q, start, sent=False):
+        line = t * starts + js
+        rising = has_above & (line <= z)
+        falling = has_below & (line >= z)
+        if sent:
+            rising = rising & (upper | (line < z))
+            falling = falling & (lower | (line > z))
+
+        @pl.when(rising)
+        def _():
+            run(last_copy(0, js, side, q, above), start)
+
+        @pl.when(falling)
+        def _():
+            run(last_copy(1, js, side, q, below), start)
+
+    def relay(ci, q, ways=(0, 1)):
         @pl.loop(0, starts)
         def _(js):
-            line = t * starts + js
-
-            if q == 0 and ci in (0, 1, 4):
-                @pl.when(line == z)
-                def _():
-                    gather_copy(order[ci][0], t).wait_recv()
-
-            @pl.when(line != z)
-            def _():
-                down_copy(0, ci, js, q, above).wait_recv()
-
-            down_onward(ci, js, q, True)
+            if 0 in ways:
+                if ci in passed and ci not in early:
+                    down_copy(0, ci, js, q, above).wait_recv()
+                else:
+                    @pl.when(t * starts + js != z)
+                    def _():
+                        down_copy(0, ci, js, q, above).wait_recv()
+
+                down_lines(ci, js, q, True)
+            if 1 in ways:
+                down_over(ci, js, q, True)
+
+    def relay_line(ci, q):
+        relay(ci, q, (0,))
+
+    def relay_over(ci, q):
+        relay(ci, q, (1,))
+
+    def last_start():
+        @pl.loop(0, starts)
+        def _(js):
+            for q in range(DOWN_CUTS):
+                down_over(finals, js, q, True)
+
+    def last_turn():
+        @pl.when(owner == t)
+        def _():
+            js = z % starts
+            for q in range(DOWN_CUTS):
+                piece = down_piece(finals, js, 1 - y, q)
+                remote(
+                    piece, piece, down_send.at[2, finals, js, q],
+                    downy_recv.at[finals, js, q], fs=across,
+                ).wait_recv()
+                last_onward(js, 1 - y, q, True)
+                last_onward(js, y, q, True, True)
+
+    def last_relay(side, q):
+        @pl.loop(0, starts)
+        def _(js):
+            @pl.when(t * starts + js != z)
+            def _():
+                last_copy(0, js, side, q, above).wait_recv()
+                last_onward(js, side, q, True, True)
 
     def relayed(ci):
         @pl.loop(0, starts)
@@ -264,10 +398,74 @@
                     fs=across,
                 ).wait_recv()
 
-    for ci in (0, 1):
-        for q in range(DOWN_CUTS):
-            relay(ci, q)
-
+    @pl.when(owner == t)
+    def _():
+        for ci in (4, 0):
+            gather_copy(order[ci][0], t).wait_recv()
+
+    @pl.when(at_end)
+    def _():
+        pass_start(0)
+        far_start()
+
+    @pl.loop(1, lines)
+    def _(d):
+        both_relay(z - d, y)
+        both_relay(z + d, y)
+        for u in range(UP_CUTS):
+            @pl.when(z - d >= 0)
+            def _():
+                up_copy(0, z - d, u, above).wait_recv()
+                up_onward(z - d, u, True)
+
+            @pl.when(z + d < lines)
+            def _():
+                up_copy(1, z + d, u, below).wait_recv()
+                up_onward(z + d, u, True)
+
+        both_relay(z - d, 1 - y)
+        both_relay(z + d, 1 - y)
+
+        for k in range(len(early)):
+            @pl.when((owner == t) & (d == k + 1))
+            def _():
+                for q in range(DOWN_CUTS):
+                    if early[k] in passed:
+                        down_copy(0, early[k], z % starts, q, above).wait_recv()
+                    down_copy(2, early[k], z % starts, q, across).start()
+
+    @pl.when(has_above & has_below)
+    def _():
+        pass_start(0)
+        far_start()
+
+    last_start()
+    inside = has_above & has_below
+    near = (lower & (z < lines // 2)) | (upper & (z >= lines // 2))
+    far = jnp.logical_not(near)
+
+    def when(condition, *moves):
+        @pl.when(condition)
+        def _():
+            for move, which, cuts in moves:
+                for q in cuts:
+                    move(which, q)
+
+    every = range(DOWN_CUTS)
+    when(inside, (pass_on, 0, every))
+
+    def share():
+        tok_copy(1, t2, t2).wait_recv()
+        tok_copy(2, t2, t1).start()
+
+    pl.when(inside)(share)
+    when(inside, (relay, 0, every))
+    when(inside & near, (relay, 1, every))
+    when(inside, (pass_on, 1, every), (relay, 2, every))
+    when(inside & near, (relay, 3, every), *((relay_line, ci, every) for ci in (4, 5, 6)))
+    pl.when(at_end)(share)
+    when(at_end & far, (relay, 0, every[:1]))
+    when(at_end & near, (pass_on, 0, every[:1]))
     tok_copy(0, t1, t1).wait_recv()
     tok_copy(2, t3, t1).wait_recv()
 
@@ -291,16 +489,29 @@
 
     width = up.shape[1]
     tiles = width // COLUMNS
-    for q in range(DOWN_CUTS):
-        relay(2, q)
-
-        @pl.loop(q * tiles // DOWN_CUTS, (q + 1) * tiles // DOWN_CUTS)
+    steps = 4
+    for k in range(steps):
+        @pl.loop(k * tiles // steps, (k + 1) * tiles // steps)
         def _(i):
             columns = pl.ds(pl.multiple_of(i * COLUMNS, COLUMNS), COLUMNS)
             before = jnp.dot(tok[...], up[:, columns], preferred_element_type=f32)
             value = jnp.maximum(before * scale[...], 0.0)
             hidden[:, columns] = (value * value).astype(bf16)
 
+        when(inside & far, (relay_line, 4 + k // 2, every[k % 2 :: 2]))
+        if k == 0:
+            when(at_end & near, (pass_on, 0, every[1:]))
+            when(at_end & far, (relay, 0, every[1:]))
+        if k == 1:
+            when(at_end & near, (relay, 0, every[:1]))
+            when(at_end & far, (relay, 1, every[:1]))
+        if k == 2:
+            when(at_end & near, (relay, 0, every[1:]))
+            when(at_end & far, (relay, 2, every[:1]))
+
+    when(at_end & far, (relay, 1, every[1:]), (relay, 2, every[1:]))
+    when((at_end & near) | (inside & far), (relay, 1, every))
+
     def product(ci):
         column, part = order[ci]
         first = pl.multiple_of(column * feats + part * half, half)
@@ -324,38 +535,46 @@
 
         cross_copy(i).start()
 
-    relay(3, 0)
+    def forward(ci):
+        when(at_end, (relay_line, ci, every))
+        for q in every:
+            relay_over(ci, q)
+
     relayed(0)
-    kept[...] = product(0)
-    for q in range(1, DOWN_CUTS):
-        relay(3, q)
+    give[0] = product(0).astype(bf16)
+    pair_copy(0).start()
+    when(inside & far, (relay_line, 6, every))
+    when(at_end & near, (pass_on, 1, every[:1]))
     relayed(1)
-    give[0] = product(1).astype(bf16)
-    pair_copy(0).start()
-    relay(4, 0)
+    kept[...] = product(1)
+    when(at_end & near, (pass_on, 1, every[1:]), (relay, 2, every))
+    when(at_end & far, (pass_on, 0, every), (pass_on, 1, every))
+    when(at_end | far, (relay, 3, every))
     cross_over(0)
-    for q in range(1, DOWN_CUTS):
-        relay(4, q)
     relayed(2)
-    kept[...] = product(2)
-    for q in range(DOWN_CUTS):
-        relay(5, q)
+    give[1] = product(2).astype(bf16)
+    pair_copy(1).start()
+    forward(4)
     relayed(3)
-    give[1] = product(3).astype(bf16)
-    pair_copy(1).start()
-    relay(6, 0)
+    kept[...] = product(3)
+    last_turn()
     cross_over(1)
-    for q in range(1, DOWN_CUTS):
-        relay(6, q)
-    for q in range(DOWN_CUTS):
-        relay(7, q)
-    for ci, i in ((4, 2), (5, 3)):
-        relayed(ci)
-        give[i] = product(ci).astype(bf16)
-        pair_copy(i).start()
+    forward(5)
+    forward(6)
+    relayed(4)
+    give[2] = product(4).astype(bf16)
+    pair_copy(2).start()
+    last_relay(y, 0)
+    last_relay(1 - y, 0)
+    relayed(5)
+    give[3] = product(5).astype(bf16)
+    pair_copy(3).start()
+    last_relay(y, 1)
+    last_relay(1 - y, 1)
+    relayed(6)
+    own[0] = product(6)
+    own[1] = product(7)
     for i in range(2):
-        relayed(6 + i)
-        own[i] = product(6 + i)
         pair_copy(2 + i).wait_recv()
         cross_copy(i).wait_recv()
 
@@ -370,11 +589,17 @@
 
     @pl.loop(0, starts)
     def _(js):
-        for ci in range(len(order)):
-            for q in range(DOWN_CUTS):
-                down_onward(ci, js, q, False)
-
-    @pl.when(owner != t)
+        for q in range(DOWN_CUTS):
+            for ci in range(len(order)):
+                if ci != finals:
+                    down_lines(ci, js, q, False)
+                down_over(ci, js, q, False)
+            for side in range(2):
+                last_onward(js, side, q, False)
+            for part in range(2):
+                pass_copies(part, js, q, False)
+
+    @pl.when((owner == t1) | (owner == t3))
     def _():
         gather_copy(t, owner).wait_send()
 
@@ -441,6 +666,7 @@
             pltpu.VMEM(down_master.shape, f32),
             pltpu.VMEM((rows, model), bf16),
             pltpu.VMEM((down_rows, feats), bf16),
+            pltpu.VMEM((starts, down_rows, feats), bf16),
             pltpu.VMEM((rows, 1), f32),
             pltpu.VMEM((rows, width), bf16),
             pltpu.VMEM((rows, half), f32),
@@ -451,6 +677,8 @@
             dma((3, lines, 2)), dma((lines, 2)),
             dma((3, 8, starts, DOWN_CUTS)),
             dma((8, starts, DOWN_CUTS)), dma((8, starts, DOWN_CUTS)),
+            dma((2, 2, starts, DOWN_CUTS)), dma((2, starts, DOWN_CUTS)),
+            dma((2, starts, 2, DOWN_CUTS)), dma((starts, 2, DOWN_CUTS)),
             dma((4,)), dma((4,)), dma((2,)), dma((2,)), dma((4,)),
         ],
         compiler_params=pltpu.CompilerParams(

time: 107 us -> 99.9 us (0.934)
  Pallas kernels: 105 us -> 97.7 us
    pallas_call x1, Pallas kernels: 102 us -> 94.1 us  [fused(): pl.pallas_call(functools.partial(kernel, n, n_tp), out_shape=(pltpu.VMEM(...]
where the time goes in v1:
time: 99.9 us; the launch traced here: 99.1 us
  Pallas kernels  97.7 us (98%)
    pallas_call x1, Pallas kernels, fused(): pl.pallas_call(functools.partial(kernel, n, n_tp), out_shape=(pltpu.VMEM(...  94.1 us
    pallas_call x1, Pallas kernels, fused(): pl.pallas_call(finish, out_shape=(jax.ShapeDtypeStruct((rows, feats), bf1...  3.64 us

profile of v1, /device:TPU:0, one launch (start us, length us, event | category | flops | bytes accessed | tf_op | source)
XLA Modules:
  0.0 99.1 jit_solution(8564649315303276908)
XLA Ops:
  0.6 0.0 copy-start
  0.6 0.7 copy-done
  1.3 94.1 %layer.1 = (bf16[2048,1024]{1,0:T(8,128)(2,1)S(1)}, bf16[1024,2048]{1,0:T(8,128)(2,1)S(1)}, f32[2,1024,256]{2,1,0:T(8,128)S(1)}, bf16[4,1024,256]{2,1,0:T(8,128)(2,1)S(1)}, bf16[2,1024,256]{2,1,0:T(8,128)(2,1)S(1)}) custom-call(bf16[1024,512]{1,0:T(8,128)(2,1)} %tokens_hbm.1, f32[1,256]{1,0:T(1,128)S(1)} %bitcast.1, f32[256,1024]{1,0:T(8,128)} %upm_hbm.1, ...), custom_call_target="tpu_custom_call" | custom-call | flops 8589934592 | bytes 16777216 | tf_op jit(solution)/shard_map/layer/pallas_call | solution.py:652
  95.4 3.6 %finish.1 = (bf16[1024,512]{1,0:T(8,128)(2,1)}, bf16[2048,1024]{1,0:T(8,128)(2,1)}, bf16[1024,2048]{1,0:T(8,128)(2,1)}) custom-call(bf16[2048,1024]{1,0:T(8,128)(2,1)S(1)} %get-tuple-element.8.up, bf16[1024,2048]{1,0:T(8,128)(2,1)S(1)} %get-tuple-element.9.down, f32[2,1024,256]{2,1,0:T(8,128)S(1)} %get-tuple-element.10.own, ...), custom_call_target="tpu_custom_call" | custom-call | tf_op jit(solution)/shard_map/finish/pallas_call | solution.py:690
Async XLA Ops:
  0.6 0.7 copy-start

commit v2 on v1

--- a/solution.py
+++ b/solution.py
@@ -12,7 +12,7 @@
 COLUMNS = 256
 BOTH = 3
 LANES = 128
-VMEM_LIMIT = 40
+VMEM_LIMIT = 46
 MIB = 1024 * 1024
 
 
@@ -20,7 +20,7 @@
     n, n_tp,
     tokens_hbm, gain_hbm, upm_hbm, downm_hbm,
     up, down, own, take, crossed,
-    gain_in, upm_in, downm_in, tok, shard, passing, scale, hidden, kept, give, cross,
+    gain_in, upm_in, downm_in, tok, shard, passing, scale, sums, hidden, kept, give, cross,
     tok_send, tok_recv, gather_send, gather_recv,
     up_send, upz_recv, upy_recv, both_send, both_recv,
     down_send, downz_recv, downy_recv, pass_send, pass_recv, last_send, last_recv,
@@ -159,9 +159,9 @@
         run(up_copy(2, line, u, across), start)
 
     both_copy(2, z, y, across).start()
-    both_onward(z, y, True)
     for u in range(UP_CUTS):
         up_onward(z, u, True)
+    both_onward(z, y, True)
 
     def gather_copy(column, to):
         return remote(
@@ -241,6 +241,7 @@
     tok_copy(1, t, t2).start()
     tok_copy(0, t, t1).start()
 
+    sums[...] = jnp.zeros(sums.shape, f32)
     both_copy(2, z, 1 - y, across).wait_recv()
     both_onward(z, 1 - y, True)
 
@@ -361,12 +362,6 @@
     def relay_over(ci, q):
         relay(ci, q, (1,))
 
-    def last_start():
-        @pl.loop(0, starts)
-        def _(js):
-            for q in range(DOWN_CUTS):
-                down_over(finals, js, q, True)
-
     def last_turn():
         @pl.when(owner == t)
         def _():
@@ -408,10 +403,84 @@
         pass_start(0)
         far_start()
 
+    rows_all, width = tok.shape[0], up.shape[1]
+    step = min(rows_all, 128)
+    low = (z < lines // 2).astype(jnp.int32)
+    final = low * (n_tp - 1)
+
+    inside = has_above & has_below
+    near = (lower & (z < lines // 2)) | (upper & (z >= lines // 2))
+    far = jnp.logical_not(near)
+
+    def share():
+        tok_copy(1, t2, t2).wait_recv()
+        tok_copy(2, t2, t1).start()
+
+    def scales():
+        @pl.loop(0, rows_all // step)
+        def _(i):
+            rows = pl.ds(pl.multiple_of(i * step, step), step)
+            values = tok[rows, :].astype(f32)
+            mean_square = jnp.mean(values * values, axis=-1, keepdims=True)
+            scale[rows, :] = lax.rsqrt(mean_square + 1e-06)
+
+    def ordered(c):
+        return low * c + (1 - low) * (n_tp - 1 - c)
+
+    def reach(c):
+        return ordered(c) * starts + starts - 1
+
+    def arrived(c):
+        @pl.loop(0, starts)
+        def _(js):
+            line = c * starts + js
+            for u in range(UP_CUTS):
+                piece = up_piece(line, 1 - y, u)
+                remote(
+                    piece, piece, up_send.at[2, line, u], upy_recv.at[line, u], fs=across
+                ).wait_recv()
+
+    def before(c, columns):
+        part = pl.ds(pl.multiple_of(c * feats, feats), feats)
+        return jnp.dot(tok[:, part], up[part, columns], preferred_element_type=f32)
+
+    def accumulate(c):
+        arrived(c)
+
+        @pl.loop(0, width // COLUMNS)
+        def _(i):
+            columns = pl.ds(pl.multiple_of(i * COLUMNS, COLUMNS), COLUMNS)
+            sums[:, columns] += before(c, columns)
+
+    def second():
+        @pl.loop(0, n_tp)
+        def _(c):
+            @pl.when(reach(c) == lines - 2)
+            def _():
+                accumulate(c)
+
     @pl.loop(1, lines)
     def _(d):
-        both_relay(z - d, y)
-        both_relay(z + d, y)
+        last = at_end & (d == lines - 1)
+
+        def reached(c, step_c):
+            @pl.loop(0, 2)
+            def _(j):
+                @pl.when(reach(c + j * step_c) <= lines - 3)
+                def _():
+                    accumulate(c + j * step_c)
+
+        @pl.when(last)
+        def _():
+            tok_copy(0, t1, t1).wait_recv()
+            reached(t, t1 - t)
+
+        @pl.when(last & far)
+        def _():
+            share()
+            tok_copy(2, t3, t1).wait_recv()
+            reached(t2, t3 - t2)
+
         for u in range(UP_CUTS):
             @pl.when(z - d >= 0)
             def _():
@@ -423,8 +492,17 @@
                 up_copy(1, z + d, u, below).wait_recv()
                 up_onward(z + d, u, True)
 
-        both_relay(z - d, 1 - y)
-        both_relay(z + d, 1 - y)
+            if u == 0:
+                @pl.when(last & far)
+                def _():
+                    second()
+                    scales()
+
+                pl.when(last & near)(share)
+
+        for column in (y, 1 - y):
+            both_relay(z - d, column)
+            both_relay(z + d, column)
 
         for k in range(len(early)):
             @pl.when((owner == t) & (d == k + 1))
@@ -439,11 +517,6 @@
         pass_start(0)
         far_start()
 
-    last_start()
-    inside = has_above & has_below
-    near = (lower & (z < lines // 2)) | (upper & (z >= lines // 2))
-    far = jnp.logical_not(near)
-
     def when(condition, *moves):
         @pl.when(condition)
         def _():
@@ -452,65 +525,68 @@
                     move(which, q)
 
     every = range(DOWN_CUTS)
+    @pl.when(owner == t)
+    def _():
+        for q in every:
+            down_over(finals, z % starts, q, True)
+
+    def all_tokens():
+        tok_copy(0, t1, t1).wait_recv()
+        tok_copy(2, t3, t1).wait_recv()
+
+    when(inside & near & (owner != t), (relay_line, 0, every), (relay_line, 2, every))
     when(inside, (pass_on, 0, every))
-
-    def share():
-        tok_copy(1, t2, t2).wait_recv()
-        tok_copy(2, t2, t1).start()
-
+    when(inside & far, (pass_on, 1, every))
     pl.when(inside)(share)
-    when(inside, (relay, 0, every))
-    when(inside & near, (relay, 1, every))
-    when(inside, (pass_on, 1, every), (relay, 2, every))
-    when(inside & near, (relay, 3, every), *((relay_line, ci, every) for ci in (4, 5, 6)))
-    pl.when(at_end)(share)
+    when(inside & near & (owner == t), (relay_line, 0, every))
+    when(inside & near, (relay_over, 0, every), (relay, 1, every))
+    pl.when(inside)(all_tokens)
+    for c in range(n_tp - 1):
+        @pl.when(inside)
+        def _():
+            accumulate(ordered(c))
+
+        when(inside & near, (pass_on, 1, every[c :: n_tp - 1]))
+    when(inside & near & (owner == t), (relay_line, 2, every))
+    when(inside & near, (relay_over, 2, every), (relay, 3, every))
+    when(inside & near, *((relay_line, ci, every) for ci in (4, 5, 6)))
+    pl.when(inside)(scales)
+    when(inside & far, (relay, 0, every))
     when(at_end & far, (relay, 0, every[:1]))
     when(at_end & near, (pass_on, 0, every[:1]))
-    tok_copy(0, t1, t1).wait_recv()
-    tok_copy(2, t3, t1).wait_recv()
-
-    rows_all = tok.shape[0]
-    step = min(rows_all, 128)
-
-    @pl.loop(0, rows_all // step)
-    def _(i):
-        rows = pl.ds(pl.multiple_of(i * step, step), step)
-        values = tok[rows, :].astype(f32)
-        mean_square = jnp.mean(values * values, axis=-1, keepdims=True)
-        scale[rows, :] = lax.rsqrt(mean_square + 1e-06)
-
-    @pl.loop(0, lines)
-    def _(line):
-        for u in range(UP_CUTS):
-            piece = up_piece(line, 1 - y, u)
-            remote(
-                piece, piece, up_send.at[2, line, u], upy_recv.at[line, u], fs=across
-            ).wait_recv()
-
-    width = up.shape[1]
+    @pl.when(at_end & near)
+    def _():
+        tok_copy(2, t3, t1).wait_recv()
+        second()
+        scales()
+
+    arrived(final)
     tiles = width // COLUMNS
     steps = 4
     for k in range(steps):
         @pl.loop(k * tiles // steps, (k + 1) * tiles // steps)
         def _(i):
             columns = pl.ds(pl.multiple_of(i * COLUMNS, COLUMNS), COLUMNS)
-            before = jnp.dot(tok[...], up[:, columns], preferred_element_type=f32)
-            value = jnp.maximum(before * scale[...], 0.0)
+            value = jnp.maximum((sums[:, columns] + before(final, columns)) * scale[...], 0.0)
             hidden[:, columns] = (value * value).astype(bf16)
 
-        when(inside & far, (relay_line, 4 + k // 2, every[k % 2 :: 2]))
         if k == 0:
+            when(inside & far, (relay, 2, every[:1]))
             when(at_end & near, (pass_on, 0, every[1:]))
             when(at_end & far, (relay, 0, every[1:]))
         if k == 1:
+            when(inside & far, (relay, 2, every[1:]))
             when(at_end & near, (relay, 0, every[:1]))
             when(at_end & far, (relay, 1, every[:1]))
         if k == 2:
+            when(inside & far, (relay_line, 4, every[:1]))
             when(at_end & near, (relay, 0, every[1:]))
             when(at_end & far, (relay, 2, every[:1]))
 
     when(at_end & far, (relay, 1, every[1:]), (relay, 2, every[1:]))
+    when(inside & far, (relay_line, 4, every[1:]))
     when((at_end & near) | (inside & far), (relay, 1, every))
+    pl.when(at_end)(last_turn)
 
     def product(ci):
         column, part = order[ci]
@@ -540,14 +616,52 @@
         for q in every:
             relay_over(ci, q)
 
+    def drain_up():
+        @pl.loop(0, lines)
+        def _(line):
+            for u in range(UP_CUTS):
+                up_onward(line, u, False)
+            for column in range(2):
+                both_onward(line, column, False)
+
+        both_copy(2, z, y, across).wait_send()
+
+        @pl.loop(0, starts)
+        def _(js):
+            for q in range(DOWN_CUTS):
+                for part in range(2):
+                    pass_copies(part, js, q, False)
+
+        @pl.when((owner == t1) | (owner == t3))
+        def _():
+            gather_copy(t, owner).wait_send()
+
+        tok_copy(0, t, t1).wait_send()
+        tok_copy(1, t, t2).wait_send()
+        tok_copy(2, t2, t1).wait_send()
+
+    def drain_down(which):
+        @pl.loop(0, starts)
+        def _(js):
+            for q in range(DOWN_CUTS):
+                for ci in which:
+                    if ci != finals:
+                        down_lines(ci, js, q, False)
+                    else:
+                        for side in range(2):
+                            last_onward(js, side, q, False)
+                    down_over(ci, js, q, False)
+
     relayed(0)
     give[0] = product(0).astype(bf16)
     pair_copy(0).start()
-    when(inside & far, (relay_line, 6, every))
-    when(at_end & near, (pass_on, 1, every[:1]))
+    when(inside & far, (relay_line, 5, every))
+    when(at_end & near, (pass_on, 1, every))
     relayed(1)
     kept[...] = product(1)
-    when(at_end & near, (pass_on, 1, every[1:]), (relay, 2, every))
+    when(inside & far, (relay_line, 6, every), (last_relay, y, every))
+    when(inside & near, *((last_relay, side, every) for side in (y, 1 - y)))
+    when(at_end & near, (relay, 2, every))
     when(at_end & far, (pass_on, 0, every), (pass_on, 1, every))
     when(at_end | far, (relay, 3, every))
     cross_over(0)
@@ -555,57 +669,33 @@
     give[1] = product(2).astype(bf16)
     pair_copy(1).start()
     forward(4)
+    pl.when(inside)(last_turn)
+    when(inside & far, (last_relay, 1 - y, every))
     relayed(3)
     kept[...] = product(3)
-    last_turn()
     cross_over(1)
     forward(5)
     forward(6)
     relayed(4)
     give[2] = product(4).astype(bf16)
     pair_copy(2).start()
-    last_relay(y, 0)
-    last_relay(1 - y, 0)
+    when(at_end, (last_relay, y, (0,)))
+    when(at_end, (last_relay, 1 - y, (0,)))
     relayed(5)
     give[3] = product(5).astype(bf16)
     pair_copy(3).start()
-    last_relay(y, 1)
-    last_relay(1 - y, 1)
+    when(at_end, (last_relay, y, (1,)))
+    when(at_end, (last_relay, 1 - y, (1,)))
+    drain_up()
+    drain_down(range(6))
+    own[1] = product(7)
     relayed(6)
     own[0] = product(6)
-    own[1] = product(7)
     for i in range(2):
         pair_copy(2 + i).wait_recv()
         cross_copy(i).wait_recv()
 
-    @pl.loop(0, lines)
-    def _(line):
-        for u in range(UP_CUTS):
-            up_onward(line, u, False)
-        for column in range(2):
-            both_onward(line, column, False)
-
-    both_copy(2, z, y, across).wait_send()
-
-    @pl.loop(0, starts)
-    def _(js):
-        for q in range(DOWN_CUTS):
-            for ci in range(len(order)):
-                if ci != finals:
-                    down_lines(ci, js, q, False)
-                down_over(ci, js, q, False)
-            for side in range(2):
-                last_onward(js, side, q, False)
-            for part in range(2):
-                pass_copies(part, js, q, False)
-
-    @pl.when((owner == t1) | (owner == t3))
-    def _():
-        gather_copy(t, owner).wait_send()
-
-    tok_copy(0, t, t1).wait_send()
-    tok_copy(1, t, t2).wait_send()
-    tok_copy(2, t2, t1).wait_send()
+    drain_down(range(6, 8))
     for i in range(4):
         pair_copy(i).wait_send()
     for i in range(2):
@@ -668,6 +758,7 @@
             pltpu.VMEM((down_rows, feats), bf16),
             pltpu.VMEM((starts, down_rows, feats), bf16),
             pltpu.VMEM((rows, 1), f32),
+            pltpu.VMEM((rows, width), f32),
             pltpu.VMEM((rows, width), bf16),
             pltpu.VMEM((rows, half), f32),
             pltpu.VMEM((4, rows, half), bf16),

time: 99.9 us -> 98.2 us (0.983)
  no operation moved by 1% of the time
where the time goes in v2:
time: 98.2 us; the launch traced here: 98 us
  Pallas kernels  97.4 us (99%)
    pallas_call x1, Pallas kernels, fused(): pl.pallas_call(functools.partial(kernel, n, n_tp), out_shape=(pltpu.VMEM(...  93.8 us
    pallas_call x1, Pallas kernels, fused(): pl.pallas_call(finish, out_shape=(jax.ShapeDtypeStruct((rows, feats), bf1...  3.64 us

profile of v2, /device:TPU:0, one launch (start us, length us, event | category | flops | bytes accessed | tf_op | source)
XLA Modules:
  0.0 98.0 jit_solution(7838277940885099785)
XLA Ops:
  0.6 93.8 %layer.1 = (bf16[2048,1024]{1,0:T(8,128)(2,1)S(1)}, bf16[1024,2048]{1,0:T(8,128)(2,1)S(1)}, f32[2,1024,256]{2,1,0:T(8,128)S(1)}, bf16[4,1024,256]{2,1,0:T(8,128)(2,1)S(1)}, bf16[2,1024,256]{2,1,0:T(8,128)(2,1)S(1)}) custom-call(bf16[1024,512]{1,0:T(8,128)(2,1)} %tokens_hbm.1, f32[1,256]{1,0:T(1,128)} %bitcast.1, f32[256,1024]{1,0:T(8,128)} %upm_hbm.1, ...), custom_call_target="tpu_custom_call" | custom-call | flops 8589934592 | bytes 16777216 | tf_op jit(solution)/shard_map/layer/pallas_call | solution.py:742
  94.4 3.6 %finish.1 = (bf16[1024,512]{1,0:T(8,128)(2,1)}, bf16[2048,1024]{1,0:T(8,128)(2,1)}, bf16[1024,2048]{1,0:T(8,128)(2,1)}) custom-call(bf16[2048,1024]{1,0:T(8,128)(2,1)S(1)} %get-tuple-element.8.up, bf16[1024,2048]{1,0:T(8,128)(2,1)S(1)} %get-tuple-element.9.down, f32[2,1024,256]{2,1,0:T(8,128)S(1)} %get-tuple-element.10.own, ...), custom_call_target="tpu_custom_call" | custom-call | tf_op jit(solution)/shard_map/finish/pallas_call | solution.py:781

commit v3 on v2

--- a/solution.py
+++ b/solution.py
@@ -21,10 +21,9 @@
     tokens_hbm, gain_hbm, upm_hbm, downm_hbm,
     up, down, own, take, crossed,
     gain_in, upm_in, downm_in, tok, shard, passing, scale, sums, hidden, kept, give, cross,
-    tok_send, tok_recv, gather_send, gather_recv,
-    up_send, upz_recv, upy_recv, both_send, both_recv,
-    down_send, downz_recv, downy_recv, pass_send, pass_recv, last_send, last_recv,
-    pair_send, pair_recv, cross_send, cross_recv, local_sem,
+    tok_recv, gather_recv, up_send, upz_recv, upy_recv, both_recv,
+    down_send, downz_recv, downy_recv, pass_send, pass_recv, last_recv,
+    pair_recv, cross_recv, once_send, local_sem,
 ):
     f32, bf16 = jnp.float32, jnp.bfloat16
     f, t = lax.axis_index("fs"), lax.axis_index("tp")
@@ -44,8 +43,12 @@
 
     up_rows = upm_in.shape[0]
     down_rows = downm_in.shape[0]
-    feats = tokens_hbm.shape[1]
+    rows_all, feats = tokens_hbm.shape
     half = feats // 2
+    width = up.shape[1]
+    (up_over, down_over_send, last_over, gather_send, tok_send, pair_send, cross_send) = (
+        once_send.at[i] for i in range(7)
+    )
     dcut = down_rows // DOWN_CUTS
     first_cut = max(8, up_rows * BOTH // 128 * 8)
     ucuts = (first_cut, first_cut + (up_rows - first_cut) // 16 * 8, up_rows)
@@ -127,45 +130,50 @@
     def both_copy(way, line, column, to):
         piece = up_piece(line, column, -1)
         return remote(
-            piece, piece, both_send.at[way, line, column], both_recv.at[line, column], fs=to
+            piece, piece, up_over if way == 2 else up_send.at[way, line],
+            both_recv.at[line, column], fs=to,
         )
 
-    def run(copy, start):
-        copy.start() if start else copy.wait_send()
-
-    def both_onward(line, column, start):
+    def spent(ref, send):
+        remote(ref, ref, send, local_sem.at[0], fs=across).wait_send()
+
+    def landed(ref, recv):
+        remote(ref, ref, local_sem.at[0], recv, fs=across).wait_recv()
+
+    def both_onward(line, column):
         @pl.when(has_above & (line <= z))
         def _():
-            run(both_copy(0, line, column, above), start)
+            both_copy(0, line, column, above).start()
 
         @pl.when(has_below & (line >= z))
         def _():
-            run(both_copy(1, line, column, below), start)
+            both_copy(1, line, column, below).start()
 
     def up_copy(way, line, u, to):
         piece = up_piece(line, y, u)
-        recv = upy_recv if way == 2 else upz_recv
-        return remote(piece, piece, up_send.at[way, line, u], recv.at[line, u], fs=to)
-
-    def up_onward(line, u, start):
+        if way == 2:
+            return remote(piece, piece, up_over, upy_recv.at[line // starts], fs=to)
+        return remote(piece, piece, up_send.at[way, line], upz_recv.at[line, u], fs=to)
+
+    def up_onward(line, u):
         @pl.when(has_above & (line <= z))
         def _():
-            run(up_copy(0, line, u, above), start)
+            up_copy(0, line, u, above).start()
 
         @pl.when(has_below & (line >= z))
         def _():
-            run(up_copy(1, line, u, below), start)
-
-        run(up_copy(2, line, u, across), start)
+            up_copy(1, line, u, below).start()
+
+        up_copy(2, line, u, across).start()
 
     both_copy(2, z, y, across).start()
     for u in range(UP_CUTS):
-        up_onward(z, u, True)
-    both_onward(z, y, True)
+        up_onward(z, u)
+    both_onward(z, y)
 
     def gather_copy(column, to):
         return remote(
-            shard, down_block(f, column), gather_send.at[0], gather_recv.at[column], tp=to
+            shard, down_block(f, column), gather_send, gather_recv.at[column], tp=to
         )
 
     order = ((t3, 0), (t2, 0), (t3, 1), (t2, 1), (t1, 0), (t1, 1), (t, 0), (t, 1))
@@ -173,10 +181,12 @@
     finals = 7
     early = (0, 1, 2)
 
-    def pass_copies(part, js, q, start, ways=(0, 1)):
+    passes_down = lower & has_below
+    passes_up = upper & has_above
+
+    def pass_copies(part, js, q, ways=(0, 1)):
         line = t2 * starts + js
         row = ((line * 2 + y) % members) * down_rows + q * dcut
-        ci = passed[part]
         here = passing.at[js, pl.ds(q * dcut, dcut), pl.ds(part * half, half)]
         there = down.at[
             pl.ds(pl.multiple_of(row, dcut), dcut),
@@ -184,27 +194,24 @@
         ]
 
         def onward(to):
-            return remote(
-                here, here, pass_send.at[0, part, js, q], pass_recv.at[part, js, q], fs=to
-            )
+            remote(here, here, pass_send.at[0, js], pass_recv.at[part, js, q], fs=to).start()
 
         if 0 in ways:
-            @pl.when(lower & has_below & (line >= z))
-            def _():
-                run(onward(below), start)
-
-            @pl.when(upper & has_above & (line <= z))
-            def _():
-                run(onward(above), start)
+            @pl.when(passes_down & (line >= z))
+            def _():
+                onward(below)
+
+            @pl.when(passes_up & (line <= z))
+            def _():
+                onward(above)
 
         if 1 in ways:
             @pl.when((upper & (line <= z)) | (lower & (line >= z)))
             def _():
-                over = remote(
-                    here, there, pass_send.at[1, part, js, q], downz_recv.at[ci, js, q],
+                remote(
+                    here, there, pass_send.at[1, js], downz_recv.at[passed[part], js, q],
                     tp=t2,
-                )
-                run(over, start)
+                ).start()
 
     def pass_on(part, q):
         @pl.loop(0, starts)
@@ -214,18 +221,15 @@
             @pl.when((upper & (line < z)) | (lower & (line > z)))
             def _():
                 here = passing.at[js, pl.ds(q * dcut, dcut), pl.ds(part * half, half)]
-                remote(
-                    here, here, pass_send.at[0, part, js, q], pass_recv.at[part, js, q],
-                    fs=above,
-                ).wait_recv()
-                pass_copies(part, js, q, True)
+                landed(here, pass_recv.at[part, js, q])
+                pass_copies(part, js, q)
 
     def pass_start(way):
         @pl.when(owner == t2)
         def _():
             for part in range(2):
                 for q in range(DOWN_CUTS):
-                    pass_copies(part, z % starts, q, True, (way,))
+                    pass_copies(part, z % starts, q, (way,))
 
     @pl.when((owner == t1) | (owner == t3))
     def _():
@@ -236,20 +240,20 @@
 
     def tok_copy(way, column, to):
         piece = tok.at[:, pl.ds(pl.multiple_of(column * feats, feats), feats)]
-        return remote(piece, piece, tok_send.at[way], tok_recv.at[way], tp=to)
+        return remote(piece, piece, tok_send, tok_recv.at[way], tp=to)
 
     tok_copy(1, t, t2).start()
     tok_copy(0, t, t1).start()
 
     sums[...] = jnp.zeros(sums.shape, f32)
     both_copy(2, z, 1 - y, across).wait_recv()
-    both_onward(z, 1 - y, True)
+    both_onward(z, 1 - y)
 
     def both_relay(line, column):
         @pl.when((line >= 0) & (line < lines))
         def _():
             both_copy(0, line, column, above).wait_recv()
-            both_onward(line, column, True)
+            both_onward(line, column)
 
     def down_piece(ci, js, side, q):
         column, part = order[ci]
@@ -262,42 +266,37 @@
 
     def down_copy(way, ci, js, q, to):
         piece = down_piece(ci, js, y, q)
-        recv = downy_recv if way == 2 else downz_recv
-        return remote(
-            piece, piece, down_send.at[way, ci, js, q], recv.at[ci, js, q], fs=to
-        )
-
-    def down_lines(ci, js, q, start):
+        if way == 2:
+            send = last_over if ci == finals else down_over_send
+            return remote(piece, piece, send, downy_recv.at[ci], fs=to)
+        return remote(piece, piece, down_send.at[way, js], downz_recv.at[ci, js, q], fs=to)
+
+    def down_lines(ci, js, q):
         line = t * starts + js
         rising = has_above & (line <= z)
         falling = has_below & (line >= z)
         if ci in passed:
             rising = rising & upper
             falling = falling & lower
-        elif start:
+        else:
             rising = rising & (upper | (line < z))
             falling = falling & (lower | (line > z))
 
         @pl.when(rising)
         def _():
-            run(down_copy(0, ci, js, q, above), start)
+            down_copy(0, ci, js, q, above).start()
 
         @pl.when(falling)
         def _():
-            run(down_copy(1, ci, js, q, below), start)
-
-    def down_over(ci, js, q, start):
-        line = t * starts + js
-        if ci == finals:
-            @pl.when(line == z)
-            def _():
-                run(down_copy(2, ci, js, q, across), start)
-        elif start and ci in early:
-            @pl.when(line != z)
+            down_copy(1, ci, js, q, below).start()
+
+    def down_over(ci, js, q):
+        if ci in early:
+            @pl.when(t * starts + js != z)
             def _():
                 down_copy(2, ci, js, q, across).start()
         else:
-            run(down_copy(2, ci, js, q, across), start)
+            down_copy(2, ci, js, q, across).start()
 
     def far_start():
         js = z % starts
@@ -322,10 +321,10 @@
     def last_copy(way, js, side, q, to):
         piece = down_piece(finals, js, side, q)
         return remote(
-            piece, piece, last_send.at[way, js, side, q], last_recv.at[js, side, q], fs=to
+            piece, piece, down_send.at[way, js], last_recv.at[js, side, q], fs=to
         )
 
-    def last_onward(js, side, q, start, sent=False):
+    def last_onward(js, side, q, sent=True):
         line = t * starts + js
         rising = has_above & (line <= z)
         falling = has_below & (line >= z)
@@ -335,11 +334,11 @@
 
         @pl.when(rising)
         def _():
-            run(last_copy(0, js, side, q, above), start)
+            last_copy(0, js, side, q, above).start()
 
         @pl.when(falling)
         def _():
-            run(last_copy(1, js, side, q, below), start)
+            last_copy(1, js, side, q, below).start()
 
     def relay(ci, q, ways=(0, 1)):
         @pl.loop(0, starts)
@@ -352,9 +351,9 @@
                     def _():
                         down_copy(0, ci, js, q, above).wait_recv()
 
-                down_lines(ci, js, q, True)
+                down_lines(ci, js, q)
             if 1 in ways:
-                down_over(ci, js, q, True)
+                down_over(ci, js, q)
 
     def relay_line(ci, q):
         relay(ci, q, (0,))
@@ -366,14 +365,10 @@
         @pl.when(owner == t)
         def _():
             js = z % starts
+            landed(down.at[pl.ds(0, down_rows), pl.ds(0, half)], downy_recv.at[finals])
             for q in range(DOWN_CUTS):
-                piece = down_piece(finals, js, 1 - y, q)
-                remote(
-                    piece, piece, down_send.at[2, finals, js, q],
-                    downy_recv.at[finals, js, q], fs=across,
-                ).wait_recv()
-                last_onward(js, 1 - y, q, True)
-                last_onward(js, y, q, True, True)
+                last_onward(js, 1 - y, q, False)
+                last_onward(js, y, q)
 
     def last_relay(side, q):
         @pl.loop(0, starts)
@@ -381,17 +376,10 @@
             @pl.when(t * starts + js != z)
             def _():
                 last_copy(0, js, side, q, above).wait_recv()
-                last_onward(js, side, q, True, True)
+                last_onward(js, side, q)
 
     def relayed(ci):
-        @pl.loop(0, starts)
-        def _(js):
-            for q in range(DOWN_CUTS):
-                piece = down_piece(ci, js, 1 - y, q)
-                remote(
-                    piece, piece, down_send.at[2, ci, js, q], downy_recv.at[ci, js, q],
-                    fs=across,
-                ).wait_recv()
+        landed(down.at[pl.ds(0, starts * down_rows), pl.ds(0, half)], downy_recv.at[ci])
 
     @pl.when(owner == t)
     def _():
@@ -403,7 +391,6 @@
         pass_start(0)
         far_start()
 
-    rows_all, width = tok.shape[0], up.shape[1]
     step = min(rows_all, 128)
     low = (z < lines // 2).astype(jnp.int32)
     final = low * (n_tp - 1)
@@ -430,15 +417,10 @@
     def reach(c):
         return ordered(c) * starts + starts - 1
 
+    rest = up_rows - first_cut
+
     def arrived(c):
-        @pl.loop(0, starts)
-        def _(js):
-            line = c * starts + js
-            for u in range(UP_CUTS):
-                piece = up_piece(line, 1 - y, u)
-                remote(
-                    piece, piece, up_send.at[2, line, u], upy_recv.at[line, u], fs=across
-                ).wait_recv()
+        landed(up.at[pl.ds(0, starts * rest), :], upy_recv.at[c])
 
     def before(c, columns):
         part = pl.ds(pl.multiple_of(c * feats, feats), feats)
@@ -485,12 +467,12 @@
             @pl.when(z - d >= 0)
             def _():
                 up_copy(0, z - d, u, above).wait_recv()
-                up_onward(z - d, u, True)
+                up_onward(z - d, u)
 
             @pl.when(z + d < lines)
             def _():
                 up_copy(1, z + d, u, below).wait_recv()
-                up_onward(z + d, u, True)
+                up_onward(z + d, u)
 
             if u == 0:
                 @pl.when(last & far)
@@ -528,7 +510,7 @@
     @pl.when(owner == t)
     def _():
         for q in every:
-            down_over(finals, z % starts, q, True)
+            down_copy(2, finals, z % starts, q, across).start()
 
     def all_tokens():
         tok_copy(0, t1, t1).wait_recv()
@@ -594,12 +576,10 @@
         return jnp.dot(hidden[...], down[:, pl.ds(first, half)], preferred_element_type=f32)
 
     def pair_copy(i):
-        return remote(give.at[i], take.at[i], pair_send.at[i], pair_recv.at[i], tp=t1)
+        return remote(give.at[i], take.at[i], pair_send, pair_recv.at[i], tp=t1)
 
     def cross_copy(i):
-        return remote(
-            cross.at[i], crossed.at[i], cross_send.at[i], cross_recv.at[i], tp=t2
-        )
+        return remote(cross.at[i], crossed.at[i], cross_send, cross_recv.at[i], tp=t2)
 
     def cross_over(i):
         pair_copy(i).wait_recv()
@@ -616,41 +596,52 @@
         for q in every:
             relay_over(ci, q)
 
-    def drain_up():
+    def drain():
         @pl.loop(0, lines)
         def _(line):
-            for u in range(UP_CUTS):
-                up_onward(line, u, False)
-            for column in range(2):
-                both_onward(line, column, False)
-
-        both_copy(2, z, y, across).wait_send()
+            for way, onward in ((0, has_above & (line <= z)), (1, has_below & (line >= z))):
+                @pl.when(onward)
+                def _():
+                    spent(up.at[pl.ds(0, up_rows + first_cut), :], up_send.at[way, line])
+
+        spent(up.at[pl.ds(0, lines * rest + first_cut), :], up_over)
 
         @pl.loop(0, starts)
         def _(js):
-            for q in range(DOWN_CUTS):
-                for part in range(2):
-                    pass_copies(part, js, q, False)
+            line = t2 * starts + js
+
+            @pl.when((passes_down & (line >= z)) | (passes_up & (line <= z)))
+            def _():
+                spent(passing.at[js], pass_send.at[0, js])
+
+            @pl.when((upper & (line <= z)) | (lower & (line >= z)))
+            def _():
+                spent(passing.at[js], pass_send.at[1, js])
 
         @pl.when((owner == t1) | (owner == t3))
         def _():
-            gather_copy(t, owner).wait_send()
-
-        tok_copy(0, t, t1).wait_send()
-        tok_copy(1, t, t2).wait_send()
-        tok_copy(2, t2, t1).wait_send()
-
-    def drain_down(which):
+            spent(shard, gather_send)
+
+        spent(tok.at[:, pl.ds(0, 3 * feats)], tok_send)
+
+    def drain_down():
         @pl.loop(0, starts)
         def _(js):
-            for q in range(DOWN_CUTS):
-                for ci in which:
-                    if ci != finals:
-                        down_lines(ci, js, q, False)
-                    else:
-                        for side in range(2):
-                            last_onward(js, side, q, False)
-                    down_over(ci, js, q, False)
+            line = t * starts + js
+            for way, onward, most in (
+                (0, has_above & (line <= z), upper), (1, has_below & (line >= z), lower),
+            ):
+                for condition, pieces in ((most, 9), (jnp.logical_not(most), 7)):
+                    @pl.when(onward & condition)
+                    def _():
+                        amount = pieces * down_rows // 8
+                        spent(tok.at[pl.ds(0, amount), :], down_send.at[way, js])
+
+        spent(down.at[pl.ds(0, starts * down_rows), pl.ds(0, 7 * half)], down_over_send)
+
+        @pl.when(owner == t)
+        def _():
+            spent(down.at[pl.ds(0, down_rows), pl.ds(0, half)], last_over)
 
     relayed(0)
     give[0] = product(0).astype(bf16)
@@ -686,20 +677,35 @@
     pair_copy(3).start()
     when(at_end, (last_relay, y, (1,)))
     when(at_end, (last_relay, 1 - y, (1,)))
-    drain_up()
-    drain_down(range(6))
+    drain()
     own[1] = product(7)
-    relayed(6)
-    own[0] = product(6)
+    if down_rows % LANES == 0:
+        def partly(side):
+            def term(js):
+                part = pl.ds(
+                    pl.multiple_of((2 * js + side) * down_rows, down_rows), down_rows
+                )
+                first = pl.multiple_of(t * feats, feats)
+                return jnp.dot(
+                    hidden[:, part], down[part, pl.ds(first, half)],
+                    preferred_element_type=f32,
+                )
+
+            return sum((term(js) for js in range(1, starts)), term(0))
+
+        own[0] = partly(y)
+        relayed(6)
+        own[0] += partly(1 - y)
+    else:
+        relayed(6)
+        own[0] = product(6)
     for i in range(2):
         pair_copy(2 + i).wait_recv()
         cross_copy(i).wait_recv()
 
-    drain_down(range(6, 8))
-    for i in range(4):
-        pair_copy(i).wait_send()
-    for i in range(2):
-        cross_copy(i).wait_send()
+    drain_down()
+    spent(give, pair_send)
+    spent(cross, cross_send)
 
 
 def finish(up, down, own, take, crossed, mixed_hbm, up_hbm, down_hbm, mixed, sems):
@@ -763,14 +769,11 @@
             pltpu.VMEM((rows, half), f32),
             pltpu.VMEM((4, rows, half), bf16),
             pltpu.VMEM((2, rows, half), bf16),
-            dma((3,)), dma((3,)), dma((1,)), dma((n_tp,)),
-            dma((3, lines, UP_CUTS)), dma((lines, UP_CUTS)), dma((lines, UP_CUTS)),
-            dma((3, lines, 2)), dma((lines, 2)),
-            dma((3, 8, starts, DOWN_CUTS)),
-            dma((8, starts, DOWN_CUTS)), dma((8, starts, DOWN_CUTS)),
-            dma((2, 2, starts, DOWN_CUTS)), dma((2, starts, DOWN_CUTS)),
-            dma((2, starts, 2, DOWN_CUTS)), dma((starts, 2, DOWN_CUTS)),
-            dma((4,)), dma((4,)), dma((2,)), dma((2,)), dma((4,)),
+            dma((3,)), dma((n_tp,)),
+            dma((2, lines)), dma((lines, UP_CUTS)), dma((n_tp,)), dma((lines, 2)),
+            dma((2, starts)), dma((8, starts, DOWN_CUTS)), dma((8,)),
+            dma((2, starts)), dma((2, starts, DOWN_CUTS)), dma((starts, 2, DOWN_CUTS)),
+            dma((4,)), dma((2,)), dma((7,)), dma((4,)),
         ],
         compiler_params=pltpu.CompilerParams(
             collective_id=0, has_side_effects=True, vmem_limit_bytes=VMEM_LIMIT * MIB

time: 98.2 us -> 97.2 us (0.990)
  Pallas kernels: 97.4 us -> 96.4 us
    pallas_call x1, Pallas kernels: 93.8 us -> 92.7 us  [fused(): pl.pallas_call(functools.partial(kernel, n, n_tp), out_shape=(pltpu.VMEM(...]
where the time goes in v3:
time: 97.2 us; the launch traced here: 97 us
  Pallas kernels  96.4 us (99%)
    pallas_call x1, Pallas kernels, fused(): pl.pallas_call(functools.partial(kernel, n, n_tp), out_shape=(pltpu.VMEM(...  92.7 us
    pallas_call x1, Pallas kernels, fused(): pl.pallas_call(finish, out_shape=(jax.ShapeDtypeStruct((rows, feats), bf1...  3.64 us

profile of v3, /device:TPU:0, one launch (start us, length us, event | category | flops | bytes accessed | tf_op | source)
XLA Modules:
  0.0 97.0 jit_solution(11623492943429870750)
XLA Ops:
  0.6 92.7 %layer.1 = (bf16[2048,1024]{1,0:T(8,128)(2,1)S(1)}, bf16[1024,2048]{1,0:T(8,128)(2,1)S(1)}, f32[2,1024,256]{2,1,0:T(8,128)S(1)}, bf16[4,1024,256]{2,1,0:T(8,128)(2,1)S(1)}, bf16[2,1024,256]{2,1,0:T(8,128)(2,1)S(1)}) custom-call(bf16[1024,512]{1,0:T(8,128)(2,1)} %tokens_hbm.1, f32[1,256]{1,0:T(1,128)} %bitcast.1, f32[256,1024]{1,0:T(8,128)} %upm_hbm.1, ...), custom_call_target="tpu_custom_call" | custom-call | flops 8589934592 | bytes 16777216 | tf_op jit(solution)/shard_map/layer/pallas_call | solution.py:748
  93.4 3.6 %finish.1 = (bf16[1024,512]{1,0:T(8,128)(2,1)}, bf16[2048,1024]{1,0:T(8,128)(2,1)}, bf16[1024,2048]{1,0:T(8,128)(2,1)}) custom-call(bf16[2048,1024]{1,0:T(8,128)(2,1)S(1)} %get-tuple-element.8.up, bf16[1024,2048]{1,0:T(8,128)(2,1)S(1)} %get-tuple-element.9.down, f32[2,1024,256]{2,1,0:T(8,128)S(1)} %get-tuple-element.10.own, ...), custom_call_target="tpu_custom_call" | custom-call | tf_op jit(solution)/shard_map/finish/pallas_call | solution.py:784

commit v4 on v3

--- a/solution.py
+++ b/solution.py
@@ -14,6 +14,108 @@
 LANES = 128
 VMEM_LIMIT = 46
 MIB = 1024 * 1024
+
+
+LINE, OVER, LAST, PASS, SHARE, TOKENS, SUM, SCALE, FINAL, TURN, CROSS = range(11)
+END_OWN = (
+    ((FINAL,), (PASS, 0, 0), (TOKENS,),),
+    ((PASS, 0, 1),),
+    ((LINE, 0, 0), (OVER, 0, 0),),
+    ((LINE, 0, 1), (OVER, 0, 1),),
+    ((LINE, 1, 0), (OVER, 1, 0), (LINE, 1, 1), (OVER, 1, 1), (TURN,),),
+    ((LINE, 6, 1), (OVER, 6, 1), (PASS, 1, 0), (PASS, 1, 1),),
+    ((LINE, 2, 0), (OVER, 2, 0), (LINE, 2, 1), (OVER, 2, 1), (LINE, 3, 0),
+     (OVER, 3, 0), (LINE, 3, 1), (OVER, 3, 1), (CROSS, 0),),
+    ((LINE, 4, 0), (OVER, 4, 0), (LINE, 4, 1), (OVER, 4, 1),),
+    ((CROSS, 1), (LINE, 5, 0), (OVER, 5, 0), (LINE, 5, 1), (OVER, 5, 1),
+     (LINE, 6, 0), (OVER, 6, 0),),
+    ((LAST, 0, 0), (LAST, 1, 0),),
+    ((LAST, 0, 1), (LAST, 1, 1),),
+)
+END_NEAR = (
+    ((TOKENS,), (PASS, 0, 0),),
+    ((PASS, 0, 1),),
+    ((LINE, 0, 0), (OVER, 0, 0),),
+    ((LINE, 0, 1), (OVER, 0, 1),),
+    ((LINE, 1, 0), (OVER, 1, 0), (LINE, 1, 1), (OVER, 1, 1),),
+    ((PASS, 1, 0), (PASS, 1, 1),),
+    ((LINE, 2, 0), (OVER, 2, 0), (LINE, 2, 1), (OVER, 2, 1), (LINE, 3, 0),
+     (OVER, 3, 0), (LINE, 3, 1), (OVER, 3, 1), (CROSS, 0),),
+    ((LINE, 4, 0), (OVER, 4, 0), (LINE, 4, 1), (OVER, 4, 1),),
+    ((CROSS, 1), (LINE, 5, 0), (OVER, 5, 0), (LINE, 5, 1), (OVER, 5, 1),
+     (LINE, 6, 0), (OVER, 6, 0), (LINE, 6, 1), (OVER, 6, 1),),
+    ((LAST, 0, 0), (LAST, 1, 0),),
+    ((LAST, 0, 1), (LAST, 1, 1),),
+)
+END_FAR = (
+    ((LINE, 0, 0), (OVER, 0, 0),),
+    ((LINE, 0, 1), (OVER, 0, 1),),
+    ((LINE, 1, 0), (OVER, 1, 0),),
+    (),
+    ((LINE, 1, 1), (OVER, 1, 1), (LINE, 2, 1), (OVER, 2, 1), (LINE, 2, 0),
+     (OVER, 2, 0),),
+    (),
+    ((PASS, 0, 0), (PASS, 0, 1), (PASS, 1, 0), (PASS, 1, 1), (LINE, 3, 0),
+     (OVER, 3, 0), (LINE, 3, 1), (OVER, 3, 1), (CROSS, 0),),
+    ((LINE, 4, 0), (OVER, 4, 0), (LINE, 4, 1), (OVER, 4, 1),),
+    ((CROSS, 1), (LINE, 5, 0), (OVER, 5, 0), (LINE, 5, 1), (OVER, 5, 1),
+     (LINE, 6, 0), (OVER, 6, 0), (LINE, 6, 1), (OVER, 6, 1),),
+    ((LAST, 0, 0), (LAST, 1, 0),),
+    ((LAST, 0, 1), (LAST, 1, 1),),
+)
+IN_OWN = (
+    ((FINAL,), (PASS, 0, 0), (PASS, 0, 1), (SHARE,), (LINE, 0, 0), (LINE, 0, 1),
+     (OVER, 0, 0), (OVER, 0, 1), (LINE, 1, 0), (OVER, 1, 0), (LINE, 1, 1),
+     (OVER, 1, 1), (TOKENS,), (SUM, 0), (PASS, 1, 0), (SUM, 1), (PASS, 1, 1),
+     (SUM, 2), (LINE, 2, 0), (LINE, 2, 1), (OVER, 2, 0), (OVER, 2, 1),
+     (LINE, 3, 0), (OVER, 3, 0), (LINE, 3, 1), (OVER, 3, 1), (LINE, 4, 0),
+     (LINE, 4, 1), (LINE, 5, 0), (LINE, 5, 1), (LINE, 6, 0), (LINE, 6, 1),
+     (SCALE,),),
+    (),
+    (),
+    (),
+    (),
+    (),
+    ((LAST, 0, 0), (LAST, 0, 1), (LAST, 1, 0), (LAST, 1, 1), (CROSS, 0),),
+    ((OVER, 4, 0), (OVER, 4, 1), (TURN,),),
+    ((CROSS, 1), (OVER, 5, 0), (OVER, 5, 1), (OVER, 6, 0), (OVER, 6, 1),),
+    (),
+    (),
+)
+IN_NEAR = (
+    ((LINE, 0, 0), (LINE, 0, 1), (LINE, 2, 0), (LINE, 2, 1), (PASS, 0, 0),
+     (PASS, 0, 1), (SHARE,), (OVER, 0, 0), (OVER, 0, 1), (LINE, 1, 0),
+     (OVER, 1, 0), (LINE, 1, 1), (OVER, 1, 1), (TOKENS,), (SUM, 0), (PASS, 1, 0),
+     (SUM, 1), (SUM, 2), (PASS, 1, 1), (OVER, 2, 0), (OVER, 2, 1), (LINE, 3, 0),
+     (OVER, 3, 0), (LINE, 3, 1), (OVER, 3, 1), (LINE, 4, 0), (LINE, 4, 1),
+     (LINE, 5, 0), (LINE, 5, 1), (LINE, 6, 0), (LINE, 6, 1), (SCALE,),),
+    (),
+    (),
+    (),
+    (),
+    (),
+    ((LAST, 0, 0), (LAST, 0, 1), (LAST, 1, 0), (LAST, 1, 1), (CROSS, 0),),
+    ((OVER, 4, 0), (OVER, 4, 1),),
+    ((CROSS, 1), (OVER, 5, 0), (OVER, 5, 1), (OVER, 6, 0), (OVER, 6, 1),),
+    (),
+    (),
+)
+IN_FAR = (
+    ((PASS, 0, 0), (PASS, 0, 1), (PASS, 1, 0), (PASS, 1, 1), (SHARE,), (TOKENS,),
+     (SUM, 0), (SUM, 1), (SUM, 2), (SCALE,), (LINE, 0, 0), (OVER, 0, 0),
+     (LINE, 0, 1), (OVER, 0, 1),),
+    ((LINE, 2, 0), (OVER, 2, 0),),
+    ((LINE, 2, 1), (OVER, 2, 1),),
+    ((LINE, 4, 0),),
+    ((LINE, 4, 1), (LINE, 1, 0), (OVER, 1, 0), (LINE, 1, 1), (OVER, 1, 1),),
+    ((LINE, 5, 0), (LINE, 5, 1),),
+    ((LINE, 6, 0), (LINE, 6, 1), (LAST, 0, 0), (LAST, 0, 1), (LINE, 3, 0),
+     (OVER, 3, 0), (LINE, 3, 1), (OVER, 3, 1), (CROSS, 0),),
+    ((OVER, 4, 0), (OVER, 4, 1), (LAST, 1, 0), (LAST, 1, 1),),
+    ((CROSS, 1), (OVER, 5, 0), (OVER, 5, 1), (OVER, 6, 0), (OVER, 6, 1),),
+    (),
+    (),
+)
 
 
 def kernel(
@@ -65,7 +167,7 @@
 
     loads = [
         pltpu.make_async_copy(upm_hbm, upm_in, local_sem.at[0]),
-        pltpu.make_async_copy(gain_hbm, gain_in, local_sem.at[1]),
+        pltpu.make_async_copy(gain_hbm, gain_in.at[0], local_sem.at[1]),
         pltpu.make_async_copy(downm_hbm, downm_in, local_sem.at[2]),
         pltpu.make_async_copy(
             tokens_hbm, tok.at[:, pl.ds(pl.multiple_of(t * feats, feats), feats)],
@@ -343,7 +445,7 @@
     def relay(ci, q, ways=(0, 1)):
         @pl.loop(0, starts)
         def _(js):
-            if 0 in ways:
+            if 0 in ways or 2 in ways:
                 if ci in passed and ci not in early:
                     down_copy(0, ci, js, q, above).wait_recv()
                 else:
@@ -351,15 +453,10 @@
                     def _():
                         down_copy(0, ci, js, q, above).wait_recv()
 
+            if 0 in ways:
                 down_lines(ci, js, q)
             if 1 in ways:
                 down_over(ci, js, q)
-
-    def relay_line(ci, q):
-        relay(ci, q, (0,))
-
-    def relay_over(ci, q):
-        relay(ci, q, (1,))
 
     def last_turn():
         @pl.when(owner == t)
@@ -499,49 +596,76 @@
         pass_start(0)
         far_start()
 
-    def when(condition, *moves):
-        @pl.when(condition)
-        def _():
-            for move, which, cuts in moves:
-                for q in cuts:
-                    move(which, q)
-
     every = range(DOWN_CUTS)
-    @pl.when(owner == t)
-    def _():
+
+    def final_over():
         for q in every:
             down_copy(2, finals, z % starts, q, across).start()
+
+    def late_tokens():
+        tok_copy(2, t3, t1).wait_recv()
+        second()
+        scales()
 
     def all_tokens():
         tok_copy(0, t1, t1).wait_recv()
         tok_copy(2, t3, t1).wait_recv()
 
-    when(inside & near & (owner != t), (relay_line, 0, every), (relay_line, 2, every))
-    when(inside, (pass_on, 0, every))
-    when(inside & far, (pass_on, 1, every))
-    pl.when(inside)(share)
-    when(inside & near & (owner == t), (relay_line, 0, every))
-    when(inside & near, (relay_over, 0, every), (relay, 1, every))
-    pl.when(inside)(all_tokens)
-    for c in range(n_tp - 1):
-        @pl.when(inside)
-        def _():
-            accumulate(ordered(c))
-
-        when(inside & near, (pass_on, 1, every[c :: n_tp - 1]))
-    when(inside & near & (owner == t), (relay_line, 2, every))
-    when(inside & near, (relay_over, 2, every), (relay, 3, every))
-    when(inside & near, *((relay_line, ci, every) for ci in (4, 5, 6)))
-    pl.when(inside)(scales)
-    when(inside & far, (relay, 0, every))
-    when(at_end & far, (relay, 0, every[:1]))
-    when(at_end & near, (pass_on, 0, every[:1]))
-    @pl.when(at_end & near)
-    def _():
-        tok_copy(2, t3, t1).wait_recv()
-        second()
-        scales()
-
+    def product(ci):
+        column, part = order[ci]
+        first = pl.multiple_of(column * feats + part * half, half)
+        return jnp.dot(hidden[...], down[:, pl.ds(first, half)], preferred_element_type=f32)
+
+    def pair_copy(i):
+        return remote(give.at[i], take.at[i], pair_send, pair_recv.at[i], tp=t1)
+
+    def cross_copy(i):
+        return remote(cross.at[i], crossed.at[i], cross_send, cross_recv.at[i], tp=t2)
+
+    def cross_over(i):
+        pair_copy(i).wait_recv()
+
+        @pl.loop(0, rows_all // step)
+        def _(j):
+            rows = pl.ds(pl.multiple_of(j * step, step), step)
+            cross[i, rows, :] = (kept[rows, :] + take[i, rows, :].astype(f32)).astype(bf16)
+
+        cross_copy(i).start()
+
+    def line_in(ci, q, end):
+        relay(ci, q, (2,) if end else (0,))
+
+    actions = {
+        LINE: line_in,
+        OVER: lambda ci, q, end: relay(ci, q, (1,)),
+        LAST: lambda side, q, end: last_relay(y + side - 2 * y * side, q),
+        PASS: lambda part, q, end: pass_on(part, q),
+        SHARE: lambda end: share(),
+        TOKENS: lambda end: late_tokens() if end else all_tokens(),
+        SUM: lambda c, end: accumulate(ordered(c)),
+        SCALE: lambda end: scales(),
+        FINAL: lambda end: final_over(),
+        TURN: lambda end: last_turn(),
+        CROSS: lambda i, end: cross_over(i),
+    }
+    own_line = owner == t
+    other_line = owner != t
+    kinds = (
+        (at_end & near & own_line, END_OWN), (at_end & near & other_line, END_NEAR),
+        (at_end & far, END_FAR), (inside & near & own_line, IN_OWN),
+        (inside & near & other_line, IN_NEAR), (inside & far, IN_FAR),
+    )
+
+    def slot(s):
+        for kind, (condition, plan) in enumerate(kinds):
+            def moves():
+                for move, *args in plan[s]:
+                    actions[move](*args, kind < 3)
+
+            if plan[s]:
+                pl.when(condition)(moves)
+
+    slot(0)
     arrived(final)
     tiles = width // COLUMNS
     steps = 4
@@ -552,49 +676,7 @@
             value = jnp.maximum((sums[:, columns] + before(final, columns)) * scale[...], 0.0)
             hidden[:, columns] = (value * value).astype(bf16)
 
-        if k == 0:
-            when(inside & far, (relay, 2, every[:1]))
-            when(at_end & near, (pass_on, 0, every[1:]))
-            when(at_end & far, (relay, 0, every[1:]))
-        if k == 1:
-            when(inside & far, (relay, 2, every[1:]))
-            when(at_end & near, (relay, 0, every[:1]))
-            when(at_end & far, (relay, 1, every[:1]))
-        if k == 2:
-            when(inside & far, (relay_line, 4, every[:1]))
-            when(at_end & near, (relay, 0, every[1:]))
-            when(at_end & far, (relay, 2, every[:1]))
-
-    when(at_end & far, (relay, 1, every[1:]), (relay, 2, every[1:]))
-    when(inside & far, (relay_line, 4, every[1:]))
-    when((at_end & near) | (inside & far), (relay, 1, every))
-    pl.when(at_end)(last_turn)
-
-    def product(ci):
-        column, part = order[ci]
-        first = pl.multiple_of(column * feats + part * half, half)
-        return jnp.dot(hidden[...], down[:, pl.ds(first, half)], preferred_element_type=f32)
-
-    def pair_copy(i):
-        return remote(give.at[i], take.at[i], pair_send, pair_recv.at[i], tp=t1)
-
-    def cross_copy(i):
-        return remote(cross.at[i], crossed.at[i], cross_send, cross_recv.at[i], tp=t2)
-
-    def cross_over(i):
-        pair_copy(i).wait_recv()
-
-        @pl.loop(0, rows_all // step)
-        def _(j):
-            rows = pl.ds(pl.multiple_of(j * step, step), step)
-            cross[i, rows, :] = (kept[rows, :] + take[i, rows, :].astype(f32)).astype(bf16)
-
-        cross_copy(i).start()
-
-    def forward(ci):
-        when(at_end, (relay_line, ci, every))
-        for q in every:
-            relay_over(ci, q)
+        slot(k + 1)
 
     def drain():
         @pl.loop(0, lines)
@@ -646,37 +728,25 @@
     relayed(0)
     give[0] = product(0).astype(bf16)
     pair_copy(0).start()
-    when(inside & far, (relay_line, 5, every))
-    when(at_end & near, (pass_on, 1, every))
+    slot(5)
     relayed(1)
     kept[...] = product(1)
-    when(inside & far, (relay_line, 6, every), (last_relay, y, every))
-    when(inside & near, *((last_relay, side, every) for side in (y, 1 - y)))
-    when(at_end & near, (relay, 2, every))
-    when(at_end & far, (pass_on, 0, every), (pass_on, 1, every))
-    when(at_end | far, (relay, 3, every))
-    cross_over(0)
+    slot(6)
     relayed(2)
     give[1] = product(2).astype(bf16)
     pair_copy(1).start()
-    forward(4)
-    pl.when(inside)(last_turn)
-    when(inside & far, (last_relay, 1 - y, every))
+    slot(7)
     relayed(3)
     kept[...] = product(3)
-    cross_over(1)
-    forward(5)
-    forward(6)
+    slot(8)
     relayed(4)
     give[2] = product(4).astype(bf16)
     pair_copy(2).start()
-    when(at_end, (last_relay, y, (0,)))
-    when(at_end, (last_relay, 1 - y, (0,)))
+    slot(9)
     relayed(5)
     give[3] = product(5).astype(bf16)
     pair_copy(3).start()
-    when(at_end, (last_relay, y, (1,)))
-    when(at_end, (last_relay, 1 - y, (1,)))
+    slot(10)
     drain()
     own[1] = product(7)
     if down_rows % LANES == 0:
@@ -780,7 +850,7 @@
         ),
         cost_estimate=pl.CostEstimate(flops=flops, bytes_accessed=16 * MIB, transcendentals=0),
         name="layer",
-    )(tokens, norm_gain[None, :], up_master, down_master)
+    )(tokens, norm_gain, up_master, down_master)
     return pl.pallas_call(
         finish,
         out_shape=(

time: 97.2 us -> 95.5 us (0.983)
  Pallas kernels: 96.4 us -> 93.6 us
    pallas_call x1, Pallas kernels: 92.7 us -> 90 us  [fused(): pl.pallas_call(functools.partial(kernel, n, n_tp), out_shape=(pltpu.VMEM(...]
where the time goes in v4:
time: 95.5 us; the launch traced here: 94.4 us
  Pallas kernels  93.6 us (98%)
    pallas_call x1, Pallas kernels, fused(): pl.pallas_call(functools.partial(kernel, n, n_tp), out_shape=(pltpu.VMEM(...  90 us
    pallas_call x1, Pallas kernels, fused(): pl.pallas_call(finish, out_shape=(jax.ShapeDtypeStruct((rows, feats), bf1...  3.64 us

profile of v4, /device:TPU:0, one launch (start us, length us, event | category | flops | bytes accessed | tf_op | source)
XLA Modules:
  0.0 94.4 jit_solution(4958102575754514029)
XLA Ops:
  0.6 90.0 %layer.1 = (bf16[2048,1024]{1,0:T(8,128)(2,1)S(1)}, bf16[1024,2048]{1,0:T(8,128)(2,1)S(1)}, f32[2,1024,256]{2,1,0:T(8,128)S(1)}, bf16[4,1024,256]{2,1,0:T(8,128)(2,1)S(1)}, bf16[2,1024,256]{2,1,0:T(8,128)(2,1)S(1)}) custom-call(bf16[1024,512]{1,0:T(8,128)(2,1)} %tokens_hbm.1, f32[256]{0:T(256)} %gain_hbm.1, f32[256,1024]{1,0:T(8,128)} %upm_hbm.1, ...), custom_call_target="tpu_custom_call" | custom-call | flops 8589934592 | bytes 16777216 | tf_op jit(solution)/shard_map/layer/pallas_call | solution.py:818
  90.6 3.6 %finish.1 = (bf16[1024,512]{1,0:T(8,128)(2,1)}, bf16[2048,1024]{1,0:T(8,128)(2,1)}, bf16[1024,2048]{1,0:T(8,128)(2,1)}) custom-call(bf16[2048,1024]{1,0:T(8,128)(2,1)S(1)} %get-tuple-element.8.up, bf16[1024,2048]{1,0:T(8,128)(2,1)S(1)} %get-tuple-element.9.down, f32[2,1024,256]{2,1,0:T(8,128)S(1)} %get-tuple-element.10.own, ...), custom_call_target="tpu_custom_call" | custom-call | tf_op jit(solution)/shard_map/finish/pallas_call | solution.py:854

commit v5 on v4

--- a/solution.py
+++ b/solution.py
@@ -23,17 +23,17 @@
     ((LINE, 0, 0), (OVER, 0, 0),),
     ((LINE, 0, 1), (OVER, 0, 1),),
     ((LINE, 1, 0), (OVER, 1, 0), (LINE, 1, 1), (OVER, 1, 1), (TURN,),),
-    ((LINE, 6, 1), (OVER, 6, 1), (PASS, 1, 0), (PASS, 1, 1),),
-    ((LINE, 2, 0), (OVER, 2, 0), (LINE, 2, 1), (OVER, 2, 1), (LINE, 3, 0),
-     (OVER, 3, 0), (LINE, 3, 1), (OVER, 3, 1), (CROSS, 0),),
-    ((LINE, 4, 0), (OVER, 4, 0), (LINE, 4, 1), (OVER, 4, 1),),
+    ((LINE, 6, 1), (OVER, 6, 1), (PASS, 1, 1), (PASS, 1, 0), (LINE, 2, 0),),
+    ((LINE, 2, 1), (OVER, 2, 1), (OVER, 2, 0), (LINE, 3, 0), (OVER, 3, 0),
+     (LINE, 3, 1), (OVER, 3, 1), (CROSS, 0), (LINE, 4, 0), (OVER, 4, 0),),
+    ((LINE, 4, 1), (OVER, 4, 1),),
     ((CROSS, 1), (LINE, 5, 0), (OVER, 5, 0), (LINE, 5, 1), (OVER, 5, 1),
-     (LINE, 6, 0), (OVER, 6, 0),),
+     (LINE, 6, 0),),
     ((LAST, 0, 0), (LAST, 1, 0),),
-    ((LAST, 0, 1), (LAST, 1, 1),),
+    ((LAST, 0, 1), (LAST, 1, 1), (OVER, 6, 0),),
 )
 END_NEAR = (
-    ((TOKENS,), (PASS, 0, 0),),
+    ((PASS, 0, 0), (TOKENS,),),
     ((PASS, 0, 1),),
     ((LINE, 0, 0), (OVER, 0, 0),),
     ((LINE, 0, 1), (OVER, 0, 1),),
@@ -54,66 +54,70 @@
     (),
     ((LINE, 1, 1), (OVER, 1, 1), (LINE, 2, 1), (OVER, 2, 1), (LINE, 2, 0),
      (OVER, 2, 0),),
-    (),
-    ((PASS, 0, 0), (PASS, 0, 1), (PASS, 1, 0), (PASS, 1, 1), (LINE, 3, 0),
-     (OVER, 3, 0), (LINE, 3, 1), (OVER, 3, 1), (CROSS, 0),),
-    ((LINE, 4, 0), (OVER, 4, 0), (LINE, 4, 1), (OVER, 4, 1),),
+    ((LINE, 4, 0),),
+    ((PASS, 0, 0), (PASS, 0, 1), (PASS, 1, 0), (PASS, 1, 1), (CROSS, 0),
+     (LINE, 3, 0), (OVER, 3, 0), (LINE, 3, 1), (OVER, 3, 1),),
+    ((OVER, 4, 0), (LINE, 4, 1), (OVER, 4, 1),),
     ((CROSS, 1), (LINE, 5, 0), (OVER, 5, 0), (LINE, 5, 1), (OVER, 5, 1),
      (LINE, 6, 0), (OVER, 6, 0), (LINE, 6, 1), (OVER, 6, 1),),
     ((LAST, 0, 0), (LAST, 1, 0),),
     ((LAST, 0, 1), (LAST, 1, 1),),
 )
 IN_OWN = (
-    ((FINAL,), (PASS, 0, 0), (PASS, 0, 1), (SHARE,), (LINE, 0, 0), (LINE, 0, 1),
+    ((PASS, 0, 0), (PASS, 0, 1), (SHARE,), (LINE, 0, 0), (LINE, 0, 1),
      (OVER, 0, 0), (OVER, 0, 1), (LINE, 1, 0), (OVER, 1, 0), (LINE, 1, 1),
      (OVER, 1, 1), (TOKENS,), (SUM, 0), (PASS, 1, 0), (SUM, 1), (PASS, 1, 1),
-     (SUM, 2), (LINE, 2, 0), (LINE, 2, 1), (OVER, 2, 0), (OVER, 2, 1),
-     (LINE, 3, 0), (OVER, 3, 0), (LINE, 3, 1), (OVER, 3, 1), (LINE, 4, 0),
+     (LINE, 2, 0), (LINE, 2, 1), (OVER, 2, 0), (LINE, 3, 0), (OVER, 3, 0),
+     (OVER, 2, 1), (LINE, 3, 1), (SUM, 2), (OVER, 3, 1), (LINE, 4, 1),
+     (LINE, 4, 0), (LINE, 5, 0), (LINE, 5, 1), (LINE, 6, 0), (LINE, 6, 1),
+     (SCALE,),),
+    ((FINAL,),),
+    (),
+    (),
+    ((OVER, 4, 0), (OVER, 4, 1),),
+    (),
+    ((LAST, 0, 0), (LAST, 1, 0), (LAST, 1, 1), (CROSS, 0),),
+    ((TURN,),),
+    ((CROSS, 1), (OVER, 5, 0), (OVER, 5, 1), (LAST, 0, 1), (OVER, 6, 1),
+     (OVER, 6, 0),),
+    (),
+    (),
+)
+IN_NEAR = (
+    ((LINE, 0, 0), (LINE, 2, 0), (PASS, 0, 0), (LINE, 2, 1), (LINE, 0, 1),
+     (PASS, 0, 1), (SHARE,), (OVER, 0, 0), (LINE, 1, 0), (OVER, 1, 0),
+     (LINE, 1, 1), (OVER, 1, 1), (OVER, 0, 1), (TOKENS,), (SUM, 0), (SUM, 1),
+     (PASS, 1, 1), (LINE, 3, 0), (OVER, 3, 0), (PASS, 1, 0), (LINE, 4, 0),
+     (SUM, 2), (LINE, 3, 1), (OVER, 2, 0), (OVER, 2, 1), (OVER, 3, 1),
      (LINE, 4, 1), (LINE, 5, 0), (LINE, 5, 1), (LINE, 6, 0), (LINE, 6, 1),
      (SCALE,),),
     (),
     (),
     (),
     (),
-    (),
-    ((LAST, 0, 0), (LAST, 0, 1), (LAST, 1, 0), (LAST, 1, 1), (CROSS, 0),),
-    ((OVER, 4, 0), (OVER, 4, 1), (TURN,),),
-    ((CROSS, 1), (OVER, 5, 0), (OVER, 5, 1), (OVER, 6, 0), (OVER, 6, 1),),
-    (),
-    (),
-)
-IN_NEAR = (
-    ((LINE, 0, 0), (LINE, 0, 1), (LINE, 2, 0), (LINE, 2, 1), (PASS, 0, 0),
-     (PASS, 0, 1), (SHARE,), (OVER, 0, 0), (OVER, 0, 1), (LINE, 1, 0),
-     (OVER, 1, 0), (LINE, 1, 1), (OVER, 1, 1), (TOKENS,), (SUM, 0), (PASS, 1, 0),
-     (SUM, 1), (SUM, 2), (PASS, 1, 1), (OVER, 2, 0), (OVER, 2, 1), (LINE, 3, 0),
-     (OVER, 3, 0), (LINE, 3, 1), (OVER, 3, 1), (LINE, 4, 0), (LINE, 4, 1),
-     (LINE, 5, 0), (LINE, 5, 1), (LINE, 6, 0), (LINE, 6, 1), (SCALE,),),
-    (),
-    (),
-    (),
-    (),
-    (),
-    ((LAST, 0, 0), (LAST, 0, 1), (LAST, 1, 0), (LAST, 1, 1), (CROSS, 0),),
-    ((OVER, 4, 0), (OVER, 4, 1),),
-    ((CROSS, 1), (OVER, 5, 0), (OVER, 5, 1), (OVER, 6, 0), (OVER, 6, 1),),
+    ((LAST, 0, 1),),
+    ((LAST, 0, 0), (LAST, 1, 0), (LAST, 1, 1), (CROSS, 0),),
+    (),
+    ((OVER, 4, 0), (OVER, 4, 1), (CROSS, 1), (OVER, 5, 0), (OVER, 5, 1),
+     (OVER, 6, 0), (OVER, 6, 1),),
     (),
     (),
 )
 IN_FAR = (
-    ((PASS, 0, 0), (PASS, 0, 1), (PASS, 1, 0), (PASS, 1, 1), (SHARE,), (TOKENS,),
-     (SUM, 0), (SUM, 1), (SUM, 2), (SCALE,), (LINE, 0, 0), (OVER, 0, 0),
+    ((PASS, 0, 1), (PASS, 1, 0), (PASS, 1, 1), (SHARE,), (TOKENS,), (SUM, 0),
+     (SUM, 2), (SUM, 1), (SCALE,), (PASS, 0, 0), (LINE, 0, 0), (OVER, 0, 0),
      (LINE, 0, 1), (OVER, 0, 1),),
     ((LINE, 2, 0), (OVER, 2, 0),),
     ((LINE, 2, 1), (OVER, 2, 1),),
     ((LINE, 4, 0),),
-    ((LINE, 4, 1), (LINE, 1, 0), (OVER, 1, 0), (LINE, 1, 1), (OVER, 1, 1),),
-    ((LINE, 5, 0), (LINE, 5, 1),),
+    ((LINE, 1, 0), (LINE, 4, 1), (OVER, 1, 0), (LINE, 1, 1), (OVER, 1, 1),),
+    ((LINE, 5, 0), (LINE, 5, 1), (OVER, 4, 0),),
     ((LINE, 6, 0), (LINE, 6, 1), (LAST, 0, 0), (LAST, 0, 1), (LINE, 3, 0),
      (OVER, 3, 0), (LINE, 3, 1), (OVER, 3, 1), (CROSS, 0),),
-    ((OVER, 4, 0), (OVER, 4, 1), (LAST, 1, 0), (LAST, 1, 1),),
-    ((CROSS, 1), (OVER, 5, 0), (OVER, 5, 1), (OVER, 6, 0), (OVER, 6, 1),),
-    (),
+    ((OVER, 4, 1),),
+    ((LAST, 1, 0), (CROSS, 1), (OVER, 5, 0), (OVER, 5, 1), (OVER, 6, 0),
+     (OVER, 6, 1),),
+    ((LAST, 1, 1),),
     (),
 )
 

time: 95.5 us -> 94.9 us (level)
  no operation moved by 1% of the time
where the time goes in v5:
time: 94.9 us; the launch traced here: 94.7 us
  Pallas kernels  93.9 us (99%)
    pallas_call x1, Pallas kernels, fused(): pl.pallas_call(functools.partial(kernel, n, n_tp), out_shape=(pltpu.VMEM(...  90.3 us
    pallas_call x1, Pallas kernels, fused(): pl.pallas_call(finish, out_shape=(jax.ShapeDtypeStruct((rows, feats), bf1...  3.64 us

profile of v5, /device:TPU:0, one launch (start us, length us, event | category | flops | bytes accessed | tf_op | source)
XLA Modules:
  0.0 94.7 jit_solution(6827959442578404504)
XLA Ops:
  0.6 90.3 %layer.1 = (bf16[2048,1024]{1,0:T(8,128)(2,1)S(1)}, bf16[1024,2048]{1,0:T(8,128)(2,1)S(1)}, f32[2,1024,256]{2,1,0:T(8,128)S(1)}, bf16[4,1024,256]{2,1,0:T(8,128)(2,1)S(1)}, bf16[2,1024,256]{2,1,0:T(8,128)(2,1)S(1)}) custom-call(bf16[1024,512]{1,0:T(8,128)(2,1)} %tokens_hbm.1, f32[256]{0:T(256)} %gain_hbm.1, f32[256,1024]{1,0:T(8,128)} %upm_hbm.1, ...), custom_call_target="tpu_custom_call" | custom-call | flops 8589934592 | bytes 16777216 | tf_op jit(solution)/shard_map/layer/pallas_call | solution.py:822
  90.9 3.6 %finish.1 = (bf16[1024,512]{1,0:T(8,128)(2,1)}, bf16[2048,1024]{1,0:T(8,128)(2,1)}, bf16[1024,2048]{1,0:T(8,128)(2,1)}) custom-call(bf16[2048,1024]{1,0:T(8,128)(2,1)S(1)} %get-tuple-element.8.up, bf16[1024,2048]{1,0:T(8,128)(2,1)S(1)} %get-tuple-element.9.down, f32[2,1024,256]{2,1,0:T(8,128)S(1)} %get-tuple-element.10.own, ...), custom_call_target="tpu_custom_call" | custom-call | tf_op jit(solution)/shard_map/finish/pallas_call | solution.py:858

commit v6 on v5

--- a/solution.py
+++ b/solution.py
@@ -583,6 +583,12 @@
 
                 pl.when(last & near)(share)
 
+            if u == UP_CUTS - 1:
+                @pl.when(last & near)
+                def _():
+                    tok_copy(2, t3, t1).wait_recv()
+                    scales()
+
         for column in (y, 1 - y):
             both_relay(z - d, column)
             both_relay(z + d, column)
@@ -607,9 +613,7 @@
             down_copy(2, finals, z % starts, q, across).start()
 
     def late_tokens():
-        tok_copy(2, t3, t1).wait_recv()
         second()
-        scales()
 
     def all_tokens():
         tok_copy(0, t1, t1).wait_recv()

time: 94.9 us -> 94.7 us (level)
  no operation moved by 1% of the time
where the time goes in v6:
time: 94.7 us; the launch traced here: 94.1 us
  Pallas kernels  93.3 us (99%)
    pallas_call x1, Pallas kernels, fused(): pl.pallas_call(functools.partial(kernel, n, n_tp), out_shape=(pltpu.VMEM(...  89.7 us
    pallas_call x1, Pallas kernels, fused(): pl.pallas_call(finish, out_shape=(jax.ShapeDtypeStruct((rows, feats), bf1...  3.64 us

profile of v6, /device:TPU:0, one launch (start us, length us, event | category | flops | bytes accessed | tf_op | source)
XLA Modules:
  0.0 94.1 jit_solution(6785797499204422984)
XLA Ops:
  0.6 89.7 %layer.1 = (bf16[2048,1024]{1,0:T(8,128)(2,1)S(1)}, bf16[1024,2048]{1,0:T(8,128)(2,1)S(1)}, f32[2,1024,256]{2,1,0:T(8,128)S(1)}, bf16[4,1024,256]{2,1,0:T(8,128)(2,1)S(1)}, bf16[2,1024,256]{2,1,0:T(8,128)(2,1)S(1)}) custom-call(bf16[1024,512]{1,0:T(8,128)(2,1)} %tokens_hbm.1, f32[256]{0:T(256)} %gain_hbm.1, f32[256,1024]{1,0:T(8,128)} %upm_hbm.1, ...), custom_call_target="tpu_custom_call" | custom-call | flops 8589934592 | bytes 16777216 | tf_op jit(solution)/shard_map/layer/pallas_call | solution.py:826
  90.3 3.6 %finish.1 = (bf16[1024,512]{1,0:T(8,128)(2,1)}, bf16[2048,1024]{1,0:T(8,128)(2,1)}, bf16[1024,2048]{1,0:T(8,128)(2,1)}) custom-call(bf16[2048,1024]{1,0:T(8,128)(2,1)S(1)} %get-tuple-element.8.up, bf16[1024,2048]{1,0:T(8,128)(2,1)S(1)} %get-tuple-element.9.down, f32[2,1024,256]{2,1,0:T(8,128)S(1)} %get-tuple-element.10.own, ...), custom_call_target="tpu_custom_call" | custom-call | tf_op jit(solution)/shard_map/finish/pallas_call | solution.py:862
